TPU v7x, 512 devices: a 8x2x16 block of a 8x8x16 slice. The times are simulated.
512 devices in a mesh: grp: 2 (over y), sp: 16 (over z), tp: 16 (over x, core).
Axes of the slice: x: 8, y: 2, z: 16, core: 2. Of those that a mesh axis runs over, the one named last changes fastest.
The devices are a block of a 8x8x16 slice.
Arguments:
- latent: bfloat16 [16384, 2048], P(('grp', 'sp', 'tp')), parts along dimension 0, may hold values from -3 to 3
- context: bfloat16 [1024, 2048], P(('grp', 'sp')), parts along dimension 0, may hold values from -6 to 6
- condition: float32 [4096], P(('grp', 'sp')), parts along dimension 0, may hold values from -6 to 6
- context_condition: float32 [2048], P('sp'), may hold values from -6 to 6
- mod_weight: bfloat16 [2048, 6144], P('sp', 'tp'), may hold values from -0.1875 to 0.1875
- mod_bias: float32 [6144], replicated, may hold values from -1.5 to 1.5
- query_weight: bfloat16 [2048, 1024], P('sp'), may hold values from -0.125 to 0.125
- key_weight: bfloat16 [2048, 1024], P('sp'), may hold values from -0.125 to 0.125
- value_weight: bfloat16 [2048, 2048], P(None, 'tp'), may hold values from -3 to 3
- out_gate_weight: bfloat16 [2048, 2048], P(None, 'tp'), may hold values from -0.125 to 0.125
- decay_in_weight: bfloat16 [2048, 32], replicated, may hold values from -0.125 to 0.125
- decay_weight: bfloat16 [2, 16, 1024], replicated, may hold values from -1.5 to 1.5
- decay_bias: float32 [2, 1024], replicated, may hold values from 0.5 to 11
- extra_decay: float32 [2, 4, 8192], P(None, None, 'sp'), may hold values from -2.1 to 0
- norm_gain: float32 [512], replicated, may hold values from 0.1 to 1.9
- out_weight: bfloat16 [2048, 2048], P('tp'), may hold values from -0.25 to 0.25
- final_gain: float32 [2048], replicated, may hold values from 0.1 to 1.9
- final_bias: float32 [2048], replicated, may hold values from -1.5 to 1.5
Outputs:
- output: bfloat16 [16384, 2048], P(('grp', 'sp', 'tp')), parts along dimension 0
There are 2 independent parts, one for each index of `grp`. A program takes and returns all parts, laid end to end along the dimension named above; an argument that names none is the same for every part. Nothing has to cross between parts.
All inputs are finite; a program needn't handle non-finite values.
Results may differ from a plain program's by a relative error of at most 0.012.
The roundings to bfloat16 on the way count: a program that leaves them out, or rounds other values in their place, can miss the bound.
Values may be sent and summed in bfloat16 or wider, within the bound.
A program may use at most 64 MiB of HBM per device.

v0:
```python
import jax
import jax.numpy as jnp
from jax import lax
from jax.sharding import PartitionSpec as P

ATTENTION_HEADS = 4
DV = 512
BLOCK = 64
GRID_W = 64


norm_eps = 1e-05
gate_scale = 16.0
rope_base = 10000.0
residual_scale = 2.0**0.5
highest = lax.Precision.HIGHEST


def sent_to_all(shard, axis):
    copies = jnp.broadcast_to(shard, (lax.axis_size(axis), *shard.shape))
    return lax.all_to_all(copies, axis, split_axis=0, concat_axis=0, tiled=True)


def over_copies(shard, axis):
    return sent_to_all(shard, axis).sum(axis=0)


def side_by_side(arrays, axis, dim, along):
    ends, at = ([], 0)
    for a in arrays[:-1]:
        at += a.shape[along]
        ends.append(at)
    both = jnp.concatenate(arrays, axis=along)
    return tuple(jnp.split(lax.all_gather(both, axis, axis=dim, tiled=True), ends, axis=along))


def in_order(pieces, dim):
    shape = list(pieces.shape[1:])
    shape[dim] *= pieces.shape[0]
    return jnp.moveaxis(pieces, 0, dim).reshape(shape)


def gathered_copies(shard, axis, dim):
    pieces = sent_to_all(shard, axis)
    return in_order(pieces, dim)


def entering(part, axis, combine, identity, reverse):
    count = lax.axis_size(axis)
    place = lax.axis_index(axis)
    ahead = count - 1 - place if reverse else place
    gathered = jax.tree.map(lambda a: lax.all_gather(a, axis), part)
    state = jax.tree.map(lambda a, e: jnp.zeros_like(a) + jnp.asarray(e, a.dtype), part, identity)

    def one(lap, state):
        source = count - 1 - lap if reverse else lap
        return combine(
            state, jax.tree.map(lambda a: lax.dynamic_index_in_dim(a, source, 0, False), gathered)
        )

    return lax.fori_loop(0, ahead, one, state)


def rotate_half(values, angle):
    half_width = values.shape[-1] // 2
    first_half = values[..., :half_width]
    second_half = values[..., half_width:]
    cosine = jnp.cos(angle)
    sine_part = jnp.sin(angle)
    return jnp.concatenate(
        [
            first_half * cosine - second_half * sine_part,
            first_half * sine_part + second_half * cosine,
        ],
        axis=-1,
    )


def rotary(values, token_places):
    quarter = values.shape[-1] // 4
    frequency = rope_base ** (-jnp.arange(quarter, dtype=jnp.float32) / quarter)
    row_index = (token_places // GRID_W).astype(jnp.float32)
    col_index = (token_places % GRID_W).astype(jnp.float32)
    half_width = 2 * quarter
    by_row = rotate_half(values[..., :half_width], row_index[:, None] * frequency)
    by_col = rotate_half(values[..., half_width:], col_index[:, None] * frequency)
    return jnp.concatenate([by_row, by_col], axis=-1)


def log_decays(low_rank, decay_weight, decay_bias):
    rank_width = decay_weight.shape[1]
    decay_parts = []
    for direction in range(2):
        logits = (
            jnp.dot(
                low_rank[:, direction * rank_width : (direction + 1) * rank_width],
                decay_weight[direction],
                preferred_element_type=jnp.float32,
            )
            + decay_bias[direction]
        )
        decay_parts.append(jax.nn.log_sigmoid(logits) / gate_scale)
    return decay_parts


def flip_rows(values):
    return jnp.flip(values, axis=0)


def end_state(key_rows, value_rows, logdec):
    cumulative = jnp.cumsum(logdec, axis=0)
    total_decay = cumulative[-1]
    weights = jnp.exp(total_decay - cumulative)
    return (total_decay, jnp.einsum("nd,nv->dv", key_rows * weights, value_rows, precision=highest))


def join_states(earlier, later):
    return (earlier[0] + later[0], jnp.exp(later[0])[:, None] * earlier[1] + later[1])


def blocked_scan(queries, key_rows, value_rows, logdec, start):
    block_count = queries.shape[0] // BLOCK
    lower_mask = jnp.tril(jnp.ones((BLOCK, BLOCK), dtype=bool))

    def blocks(values):
        return values.reshape(block_count, BLOCK, values.shape[1])

    def advance(carry_state, block_data):
        query_block, key_block, value_block, decay_block = block_data
        cumulative = jnp.cumsum(decay_block, axis=0)
        total_decay = cumulative[-1]
        query_decayed = query_block * jnp.exp(cumulative)
        key_inverse = key_block * jnp.exp(-cumulative)
        key_closing = key_block * jnp.exp(total_decay - cumulative)
        scores = jnp.einsum("cd,sd->cs", query_decayed, key_inverse, precision=highest)
        scores = jnp.where(lower_mask, scores, 0.0)
        outputs = jnp.einsum("cs,sv->cv", scores, value_block, precision=highest) + jnp.einsum(
            "cd,dv->cv", query_decayed, carry_state, precision=highest
        )
        carry_state = jnp.exp(total_decay)[:, None] * carry_state + jnp.einsum(
            "cd,cv->dv", key_closing, value_block, precision=highest
        )
        return (carry_state, outputs)

    unused_state, outputs = lax.scan(
        advance, start, (blocks(queries), blocks(key_rows), blocks(value_rows), blocks(logdec))
    )
    return outputs.reshape(queries.shape[0], value_rows.shape[1])


def body(
    latent,
    context,
    condition,
    context_condition,
    mod_weight,
    mod_bias,
    query_weight,
    key_weight,
    value_weight,
    out_gate_weight,
    decay_in_weight,
    decay_weight,
    decay_bias,
    extra_decay,
    norm_gain,
    out_weight,
    final_gain,
    final_bias,
):
    model_width = latent.shape[1]
    head_keys = query_weight.shape[1] // ATTENTION_HEADS
    value_cols = value_weight.shape[1]
    tp_index = lax.axis_index("tp")
    head_share = lax.axis_size("tp") // ATTENTION_HEADS
    head_index = tp_index // head_share
    part_index = tp_index % head_share
    activated = jax.nn.silu(jnp.stack([condition, context_condition])).astype(jnp.bfloat16)
    partial_value = jnp.dot(activated, mod_weight, preferred_element_type=jnp.float32)
    row_sums = over_copies(partial_value, "sp")
    modulation = lax.all_gather(row_sums, "tp", axis=1, tiled=True)
    modulation = modulation + mod_bias
    shifts = modulation[:, :model_width]
    scales = modulation[:, model_width : 2 * model_width]
    branch_gate = modulation[0, 2 * model_width :]
    mod_latent = (latent.astype(jnp.float32) * (1.0 + scales[0]) + shifts[0]).astype(jnp.bfloat16)
    mod_context = (context.astype(jnp.float32) * (1.0 + scales[1]) + shifts[1]).astype(jnp.bfloat16)
    key_start = head_index * head_keys
    query_slice = lax.dynamic_slice_in_dim(query_weight, key_start, head_keys, 1)
    key_slice = lax.dynamic_slice_in_dim(key_weight, key_start, head_keys, 1)
    query_head, key_head = side_by_side((query_slice, key_slice), "sp", 0, 1)
    combined = jnp.concatenate(
        [query_head, out_gate_weight, key_head, value_weight, decay_in_weight], axis=1
    )
    offset = head_keys + value_cols
    projected = jnp.dot(
        gathered_copies(mod_latent, "tp", 0), combined, preferred_element_type=jnp.float32
    ).astype(jnp.bfloat16)
    context_local = jnp.dot(
        mod_context, combined[:, offset:], preferred_element_type=jnp.float32
    ).astype(jnp.bfloat16)
    gathered_context = gathered_copies(context_local, "sp", 0)
    queries = projected[:, :head_keys].astype(jnp.float32) * head_keys ** (-0.5)
    out_gate = projected[:, head_keys:offset]
    key_rows = projected[:, offset : offset + head_keys].astype(jnp.float32)
    value_rows = projected[:, offset + head_keys : offset + head_keys + value_cols].astype(
        jnp.float32
    )
    low_rank = projected[:, offset + head_keys + value_cols :]
    token_places = lax.axis_index("sp") * projected.shape[0] + jnp.arange(
        projected.shape[0], dtype=jnp.int32
    )
    queries = rotary(queries, token_places)
    key_rows = rotary(key_rows, token_places)
    head_bias = lax.dynamic_slice_in_dim(decay_bias, key_start, head_keys, 1)
    head_gate = lax.dynamic_slice_in_dim(decay_weight, key_start, head_keys, 2)
    head_extra = lax.dynamic_index_in_dim(extra_decay, head_index, 1, keepdims=False)
    latent_decay = log_decays(low_rank, head_gate, head_bias)
    forward_decay = latent_decay[0] + head_extra[0][:, None]
    backward_decay = latent_decay[1] + head_extra[1][:, None]
    context_keys = gathered_context[:, :head_keys].astype(jnp.float32)
    context_values = gathered_context[:, head_keys : head_keys + value_cols].astype(jnp.float32)
    context_decay = log_decays(gathered_context[:, head_keys + value_cols :], head_gate, head_bias)
    context_forward = end_state(context_keys, context_values, context_decay[0])[1]
    context_backward = end_state(
        flip_rows(context_keys), flip_rows(context_values), flip_rows(context_decay[1])
    )[1]
    forward_total, forward_state = end_state(key_rows, value_rows, forward_decay)
    backward_total, backward_state = end_state(
        flip_rows(key_rows), flip_rows(value_rows), flip_rows(backward_decay)
    )
    identity = (
        jnp.zeros((head_keys,), jnp.float32),
        jnp.zeros((head_keys, value_cols), jnp.float32),
    )
    arrived_forward = entering((forward_total, forward_state), "sp", join_states, identity, False)
    arrived_backward = entering((backward_total, backward_state), "sp", join_states, identity, True)
    start_forward = jnp.exp(arrived_forward[0])[:, None] * context_forward + arrived_forward[1]
    start_backward = jnp.exp(arrived_backward[0])[:, None] * context_backward + arrived_backward[1]
    out_forward = blocked_scan(queries, key_rows, value_rows, forward_decay, start_forward)
    out_backward = flip_rows(
        blocked_scan(
            flip_rows(queries),
            flip_rows(key_rows),
            flip_rows(value_rows),
            flip_rows(backward_decay),
            start_backward,
        )
    )
    mixture = out_forward + out_backward
    squares = jnp.sum(mixture * mixture, axis=1)
    onehot = (jnp.arange(ATTENTION_HEADS) == head_index).astype(jnp.float32)
    totals = over_copies(onehot[:, None] * squares[None, :], "tp")
    head_sum = jnp.sum(totals * onehot[:, None], axis=0)
    gain_slice = lax.dynamic_slice_in_dim(norm_gain, part_index * value_cols, value_cols, 0)
    normed = mixture * lax.rsqrt(head_sum / DV + norm_eps)[:, None] * gain_slice
    gated_rows = (normed * jax.nn.silu(out_gate.astype(jnp.float32))).astype(jnp.bfloat16)
    regrouped = lax.all_to_all(gated_rows, "tp", split_axis=0, concat_axis=1, tiled=True)
    branch = jnp.dot(
        regrouped,
        lax.all_gather(out_weight, "tp", axis=0, tiled=True),
        preferred_element_type=jnp.float32,
    )
    summed = residual_scale * latent.astype(jnp.float32) + branch_gate * branch
    row_mean = jnp.mean(summed, axis=1, keepdims=True)
    centered = summed - row_mean
    variance = jnp.mean(centered * centered, axis=1, keepdims=True)
    return (centered * lax.rsqrt(variance + norm_eps) * final_gain + final_bias).astype(
        jnp.bfloat16
    )


def solution(mesh):
    placed = (
        P(("grp", "sp", "tp"), None),
        P(("grp", "sp"), None),
        P(("grp", "sp")),
        P("sp"),
        P("sp", "tp"),
        P(),
        P("sp", None),
        P("sp", None),
        P(None, "tp"),
        P(None, "tp"),
        P(),
        P(),
        P(),
        P(None, None, "sp"),
        P(),
        P("tp", None),
        P(),
        P(),
    )
    return jax.shard_map(
        body, mesh=mesh, in_specs=placed, out_specs=P(("grp", "sp", "tp"), None), check_vma=False
    )
```

profile of v0, /device:TPU:65, one launch (start us, length us, event | category | flops | bytes accessed | tf_op | source)
XLA Modules:
  0.0 405.9 jit_solution(8902771420306795943)
XLA Ops:
  8.9 44.2 %all-to-all-start = ((f32[16,2,384]{2,1,0:T(2,128)}), f32[16,2,384]{2,1,0:T(2,128)S(1)}, u32[]{:S(2)}, u32[]{:S(2)}) async-start(f32[16,2,384]{2,1,0:T(2,128)} %broadcast_in_dim.33), calls=%async_computation | async-start | bytes 98304 | tf_op jit(solution)/shard_map/all_to_all | solution.py:21
  54.8 9.6 %all-to-all-done = f32[16,2,384]{2,1,0:T(2,128)S(1)} async-done(((f32[16,2,384]{2,1,0:T(2,128)}), f32[16,2,384]{2,1,0:T(2,128)S(1)}, u32[]{:S(2)}, u32[]{:S(2)}) %all-to-all-start) | async-done | bytes 49184 | tf_op jit(solution)/shard_map/all_to_all | solution.py:21
  64.5 19.9 %all_gather.27 = f32[2,6144]{1,0:T(2,128)S(1)} all-gather(f32[2,384]{1,0:T(2,128)S(1)} %reduce_sum.54), channel_id=1, replica_groups=mesh['grp'=2,'sp'=16,'tp'=16] {'tp'}, dimensions={1}, use_global_device_ids=true | all-gather | bytes 52224 | tf_op jit(solution)/shard_map/all_gather | solution.py:181
  86.2 1.6 broadcast_in_dim.36
  87.8 4.5 %all-to-all-start.1 = ((bf16[16,32,2048]{2,1,0:T(8,128)(2,1)}), bf16[16,32,2048]{2,1,0:T(8,128)(2,1)S(1)}, u32[]{:S(2)}, u32[]{:S(2)}) async-start(bf16[16,32,2048]{2,1,0:T(8,128)(2,1)} %broadcast_in_dim.36), calls=%async_computation.1 | async-start | bytes 4194304 | tf_op jit(solution)/shard_map/all_to_all | solution.py:21
  94.9 29.8 %all-gather.9.cloned.1.call-done = bf16[2048,512]{1,0:T(8,128)(2,1)} async-done(((bf16[128,512]{1,0:T(8,128)(2,1)}), bf16[2048,512]{1,0:T(8,128)(2,1)}) %all-gather.9.cloned.1.call-update) | async-done | bytes 2097168 | tf_op jit(solution)/shard_map/all_gather | solution.py:34
  124.7 2.5 slice_dynamic-update-slice_fusion
  128.2 1.5 fusion.169
  131.5 9.9 %all-to-all-done.1 = bf16[16,32,2048]{2,1,0:T(8,128)(2,1)S(1)} async-done(((bf16[16,32,2048]{2,1,0:T(8,128)(2,1)}), bf16[16,32,2048]{2,1,0:T(8,128)(2,1)S(1)}, u32[]{:S(2)}, u32[]{:S(2)}) %all-to-all-start.1) | async-done | bytes 2097184 | tf_op jit(solution)/shard_map/all_to_all | solution.py:21
  141.4 4.0 convolution_convert_fusion
  146.3 1.2 fusion.86
  149.5 1.9 fusion.133
  153.2 1.3 fusion.95
  154.6 2.1 fusion.78
  160.0 1.3 copy.119
  161.5 2.2 fusion.102
  163.8 1.8 fusion.73
  166.5 4.0 all-to-all-start.2
  174.9 3.0 rev.35
  179.2 39.7 %all-gather.3 = f32[16,1,256]{2,1,0:T(1,128)S(1)} all-gather(f32[1,1,256]{2,1,0:T(1,128)S(1)} %bitcast.358), channel_id=1, replica_groups=mesh['grp'=2,'sp'=16,'tp'=16] {'sp'}, dimensions={0}, use_global_device_ids=true | all-gather | bytes 17408 | tf_op jit(solution)/shard_map/all_gather | solution.py:52
  218.9 1.2 copy.136
  220.2 21.6 %all-gather.2 = f32[16,1,256]{2,1,0:T(1,128)S(1)} all-gather(f32[1,1,256]{2,1,0:T(1,128)S(1)} %bitcast.363), channel_id=1, replica_groups=mesh['grp'=2,'sp'=16,'tp'=16] {'sp'}, dimensions={0}, use_global_device_ids=true | all-gather | bytes 17408 | tf_op jit(solution)/shard_map/all_gather | solution.py:52
  241.8 1.4 fusion.83
  244.2 2.1 fusion.87
  247.1 2.0 fusion.80
  249.2 3.8 reverse.3
  253.8 1.2 reshape.298
  258.8 4.8 %rev.32 = f32[512,256]{1,0:T(8,128)} reverse(f32[512,256]{1,0:T(8,128)} %slice_convert_fusion), dimensions={0} | reverse | bytes 1048576 | tf_op jit(solution)/shard_map/jit(_flip)/rev | solution.py:107
  263.6 1.3 rev.34
  264.9 2.0 reshape.289
  266.9 2.1 copy.121
  270.5 16.3 %while.53 = (s32[]{:T(128)}, f32[256]{0:T(256)S(1)}, f32[256,128]{1,0:T(8,128)S(1)}, s32[]{:T(128)}, f32[16,256]{1,0:T(8,128)S(1)}, /*index=5*/f32[16,256,128]{2...) while((s32[]{:T(128)}, f32[256]{0:T(256)S(1)}, f32[256,128]{1,0:T(8,128)S(1)}, s32[]{:T(128)}, ...), condition=%wide.region_13.14_spmd, body=%wide.region_12.13_spmd.sunk | while | flops 65798 | bytes 400539 | solution.py:61
  286.7 2.3 fusion.71
  289.8 33.4 %while.55 = (s32[]{:T(128)}, f32[256,128]{1,0:T(8,128)S(1)}, f32[8,64,128]{2,1,0:T(8,128)}, f32[8,64,256]{2,1,0:T(8,128)}, f32[8,64,256]{2,1,0:T(8,128)S(1)}, /*...) while((s32[]{:T(128)}, f32[256,128]{1,0:T(8,128)S(1)}, ...), condition=%wide.region_18.19_spmd.clone, body=%wide.region_16.18_spmd.clone.sunk | while | flops 70418432 | bytes 1386085 | solution.py:145
  296.9 1.2 convolution_add_fusion.11
  325.4 28.7 %while.54 = (s32[]{:T(128)}, f32[256,128]{1,0:T(8,128)S(1)}, f32[8,64,128]{2,1,0:T(8,128)S(1)}, f32[8,64,256]{2,1,0:T(8,128)}, f32[8,64,256]{2,1,0:T(8,128)S(1)}...) while((s32[]{:T(128)}, f32[256,128]{1,0:T(8,128)S(1)}, ...), condition=%wide.region_9.10_spmd.clone, body=%wide.region_7.9_spmd.clone.sunk | while | flops 70418432 | bytes 1386085 | solution.py:145
  327.8 1.2 convolution_add_fusion.10
  331.4 1.2 convolution_add_fusion.10
  335.0 1.2 convolution_add_fusion.10
  338.5 1.2 convolution_add_fusion.10
  342.1 1.2 convolution_add_fusion.10
  345.7 1.2 convolution_add_fusion.10
  349.3 1.2 convolution_add_fusion.10
  352.9 1.2 convolution_add_fusion.10
  355.0 16.5 %all-to-all-start.3 = ((f32[16,4,512]{2,1,0:T(4,128)}), f32[16,4,512]{2,1,0:T(4,128)S(1)}, u32[]{:S(2)}, u32[]{:S(2)}) async-start(f32[16,4,512]{2,1,0:T(4,128)} %broadcast_in_dim.38), calls=%async_computation.3 | async-start | bytes 262144 | tf_op jit(solution)/shard_map/all_to_all | solution.py:21
  372.3 8.1 %all-to-all-done.3 = f32[16,4,512]{2,1,0:T(4,128)S(1)} async-done(((f32[16,4,512]{2,1,0:T(4,128)}), f32[16,4,512]{2,1,0:T(4,128)S(1)}, u32[]{:S(2)}, u32[]{:S(2)}) %all-to-all-start.3) | async-done | bytes 131104 | tf_op jit(solution)/shard_map/all_to_all | solution.py:21
  381.7 11.6 %all_to_all.39 = bf16[16,32,128]{2,1,0:T(8,128)(2,1)S(1)} all-to-all(bf16[16,32,128]{2,1,0:T(8,128)(2,1)S(1)} %bitcast.340), channel_id=1, replica_groups=mesh['grp'=2,'sp'=16,'tp'=16] {'tp'}, dimensions={0} | all-to-all | bytes 262144 | tf_op jit(solution)/shard_map/all_to_all | solution.py:258
  393.3 5.1 %fusion.172 = (f32[32]{0:T(128)S(1)}, f32[32,2048]{1,0:T(8,128)S(1)}) fusion(bf16[2048,2048]{1,0:T(8,128)(2,1)} %all-gather.11.cloned.1.call-done, f32[2048]{0:T(1024)S(1)} %bitcast.349, bf16[32,2048]{1,0:T(8,128)(2,1)S(1)} %copy-done.10, bf16[16,32,128]{2,1,0:T(8,128)(2,1)S(1)} %all_to_all.39), kind=kOutput, calls=%fused_computation.264 | convolution fusion | flops 268763104 | bytes 8921216 | tf_op jit(solution)/shard_map/dot_general | solution.py:259
  (314 shorter events, 106.7 us)
Async XLA Ops:
  6.5 0.9 copy-start
  8.9 55.6 %all-to-all-start = ((f32[16,2,384]{2,1,0:T(2,128)}), f32[16,2,384]{2,1,0:T(2,128)S(1)}, u32[]{:S(2)}, u32[]{:S(2)}) async-start(f32[16,2,384]{2,1,0:T(2,128)} %broadcast_in_dim.33), calls=%async_computation | async-start | bytes 98304 | tf_op jit(solution)/shard_map/all_to_all | solution.py:21
  53.1 71.6 %all-gather.9.cloned.1.call-start = ((), (), s32[]{:S(2)}) async-start(), calls=%async_computation.5 | async-start | bytes 2228224 | tf_op jit(solution)/shard_map/all_gather | solution.py:34
  54.1 38.3 %copy-start.11 = (bf16[2048,32]{0,1:T(8,128)(2,1)S(1)}, bf16[2048,32]{0,1:T(8,128)(2,1)}, u32[]{:S(2)}) copy-start(bf16[2048,32]{0,1:T(8,128)(2,1)} %param.36) | copy-start | bytes 393220
  87.8 39.5 %copy-start.6 = (bf16[2048,128]{1,0:T(8,128)(2,1)S(1)}, bf16[2048,128]{1,0:T(8,128)(2,1)}, u32[]{:S(2)}) copy-start(bf16[2048,128]{1,0:T(8,128)(2,1)} %param.35) | copy-start | bytes 1572868
  87.8 53.6 %all-to-all-start.1 = ((bf16[16,32,2048]{2,1,0:T(8,128)(2,1)}), bf16[16,32,2048]{2,1,0:T(8,128)(2,1)S(1)}, u32[]{:S(2)}, u32[]{:S(2)}) async-start(bf16[16,32,2048]{2,1,0:T(8,128)(2,1)} %broadcast_in_dim.36), calls=%async_computation.1 | async-start | bytes 4194304 | tf_op jit(solution)/shard_map/all_to_all | solution.py:21
  92.3 178.1 %all-gather.15.cloned.1.call-start = ((), (), s32[]{:S(2)}) async-start(), calls=%async_computation.8 | async-start | bytes 2228224 | tf_op jit(solution)/shard_map/all_gather | solution.py:52
  92.7 37.9 %copy-start.3 = (bf16[2048,32]{1,0:T(8,128)(2,1)}, bf16[2048,32]{1,0:T(8,128)(2,1)S(1)}, u32[]{:S(2)}) copy-start(bf16[2048,32]{1,0:T(8,128)(2,1)S(1)} %copy.116) | copy-start | bytes 393220
  94.1 51.4 %copy-start.15 = (f32[1,256]{1,0:T(1,128)}, f32[1,256]{1,0:T(1,128)S(1)}, u32[]{:S(2)}) copy-start(f32[1,256]{1,0:T(1,128)S(1)} %get-tuple-element.335) | copy-start | bytes 3076
  124.7 3.5 copy-start.2
  124.7 5.0 %copy-start.7 = (bf16[2048,128]{1,0:T(8,128)(2,1)S(1)}, bf16[2048,128]{1,0:T(8,128)(2,1)}, u32[]{:S(2)}) copy-start(bf16[2048,128]{1,0:T(8,128)(2,1)} %param.34) | copy-start | bytes 1572868
  145.4 0.9 copy-start.5
  147.5 2.0 copy-start.17
  151.4 0.7 copy-start.8
  151.4 0.7 copy-start.9
  154.6 170.1 %all-gather.13.cloned.1.call-start = ((), (), s32[]{:S(2)}) async-start(), calls=%async_computation.7 | async-start | bytes 2228224 | tf_op jit(solution)/shard_map/all_gather | solution.py:52
  156.9 6.9 %copy-start.4 = (bf16[2048,32]{1,0:T(8,128)(2,1)S(1)}, bf16[2048,32]{1,0:T(8,128)(2,1)}, u32[]{:S(2)}) copy-start(bf16[2048,32]{1,0:T(8,128)(2,1)} %copy-done.3) | copy-start | bytes 393220
  166.5 77.7 %all-to-all-start.2 = ((bf16[16,32,416]{2,1,0:T(8,128)(2,1)}), bf16[16,32,416]{2,1,0:T(8,128)(2,1)S(1)}, u32[]{:S(2)}, u32[]{:S(2)}) async-start(bf16[16,32,416]{2,1,0:T(8,128)(2,1)} %broadcast_in_dim.37), calls=%async_computation.2 | async-start | bytes 1048576 | tf_op jit(solution)/shard_map/all_to_all | solution.py:21
  170.5 222.8 %all-gather.11.cloned.1.call-start = ((), (), s32[]{:S(2)}) async-start(), calls=%async_computation.6 | async-start | bytes 8912896 | tf_op jit(solution)/shard_map/all_gather | solution.py:261
  174.9 69.3 %copy-start.16 = (f32[1,256]{1,0:T(1,128)S(1)}, f32[1,256]{1,0:T(1,128)}, u32[]{:S(2)}) copy-start(f32[1,256]{1,0:T(1,128)} %copy-done.15) | copy-start | bytes 3076
  258.7 8.2 %copy-start.1 = (f32[256,4,128]{0,2,1:T(8,128)}, f32[256,4,128]{0,2,1:T(8,128)S(1)}, u32[]{:S(2)}) copy-start(f32[256,4,128]{0,2,1:T(8,128)S(1)} %copy.132) | copy-start | bytes 1572868
  325.3 28.9 %copy-start.14 = (f32[4]{0:T(128)S(1)}, f32[4]{0:T(128)}, u32[]{:S(2)}) copy-start(f32[4]{0:T(128)} %compare_convert_fusion) | copy-start | bytes 52
  325.4 67.9 %copy-start.10 = (bf16[32,2048]{1,0:T(8,128)(2,1)S(1)}, bf16[32,2048]{1,0:T(8,128)(2,1)}, u32[]{:S(2)}) copy-start(bf16[32,2048]{1,0:T(8,128)(2,1)} %param.26) | copy-start | bytes 393220
  355.0 25.4 %all-to-all-start.3 = ((f32[16,4,512]{2,1,0:T(4,128)}), f32[16,4,512]{2,1,0:T(4,128)S(1)}, u32[]{:S(2)}, u32[]{:S(2)}) async-start(f32[16,4,512]{2,1,0:T(4,128)} %broadcast_in_dim.38), calls=%async_computation.3 | async-start | bytes 262144 | tf_op jit(solution)/shard_map/all_to_all | solution.py:21
  393.3 5.3 %copy-start.12 = (f32[2048]{0:T(1024)S(1)}, f32[2048]{0:T(1024)}, u32[]{:S(2)}) copy-start(f32[2048]{0:T(1024)} %param.43) | copy-start | bytes 24580
  393.3 5.3 %copy-start.13 = (f32[2048]{0:T(1024)S(1)}, f32[2048]{0:T(1024)}, u32[]{:S(2)}) copy-start(f32[2048]{0:T(1024)} %param.42) | copy-start | bytes 24580
Sparse Core Ops, SparseCore 0:
  56.0 68.6 all-gather.8
  154.7 77.2 all-gather.14
  234.1 68.7 all-gather.12
  304.9 67.7 all-gather.10
where the time goes:
time: 411 us; the launch traced here: 406 us
  blocking collectives  92.8 us (23%)
  matrix products  71.4 us (17%)
  starting transfers between devices  69.5 us (17%)
  local copies, waits for them, and re-layouts  64.1 us (16%)
  waiting for transfers between devices  58.2 us (14%)
  other arithmetic  34.7 us (8%)
  between operations  13.8 us (3%)
    all_to_all x4, starting transfers between devices, sent_to_all(): return lax.all_to_all(copies, axis, split_axis=0, concat_axis=0, tiled=True)  69.3 us
    all_gather x2, blocking collectives, entering(): gathered = jax.tree.map(lambda a: lax.all_gather(a, axis), part)  61.3 us
    all_gather x1, waiting for transfers between devices, side_by_side(): lax.all_gather(both, axis, axis=dim, tiled=True)  29.8 us
    all_to_all x4, waiting for transfers between devices, sent_to_all(): return lax.all_to_all(copies, axis, split_axis=0, concat_axis=0, tiled=True)  27.6 us
    all_gather x1, blocking collectives, body(): modulation = lax.all_gather(row_sums, 'tp', axis=1, tiled=True)  19.9 us
    dot_general x16, matrix products, advance(): jnp.einsum('cd,cv->dv', key_closing, value_block, precision=highest)  19.1 us
    add x15, other arithmetic, join_states(): jnp.exp(later[0])[:, None] * earlier[1] + later[1]  15.3 us
    dot_general x16, matrix products, advance(): jnp.einsum('cs,sv->cv', scores, value_block, precision=highest)  14.8 us
  transfers between devices with their start and end apart: 8, of which 4 were waited for; matrix products, arithmetic and copies ran while one was open for 37% of the time, Pallas kernels for 0%

commit v1 on v0

v1 whole, which is shorter than its diff:
```python
import functools

import numpy as np
import jax
import jax.numpy as jnp
from jax import lax
from jax.experimental import pallas as pl
from jax.experimental.pallas import tpu as pltpu
from jax.sharding import PartitionSpec as P

ATTENTION_HEADS = 4
DV = 512
BLOCK = 64
GRID_W = 64

norm_eps = 1e-05
gate_scale = 16.0
rope_base = 10000.0
residual_scale = 2.0**0.5
highest = lax.Precision.HIGHEST
f32 = jnp.float32
bf16 = jnp.bfloat16

NT = (((1,), (1,)), ((), ()))
TN = (((0,), (0,)), ((), ()))


def dot(a, b, dims=None, precision=None):
    if dims is None:
        dims = (((1,), (0,)), ((), ()))
    return lax.dot_general(a, b, dims, precision=precision, preferred_element_type=f32)


def log_sigmoid(v):
    return jnp.minimum(v, 0.0) - jnp.log1p(jnp.exp(-jnp.abs(v)))


def silu(v):
    return v / (1.0 + jnp.exp(-v))


def rotary_tables(rows, half):
    quarter = half // 2
    frequency = (rope_base ** (-np.arange(quarter, dtype=np.float64) / quarter)).astype(np.float32)

    def table(places):
        angle = (np.arange(places, dtype=np.float32)[:, None] * frequency).astype(np.float64)
        cosine = np.cos(angle)
        sine = np.sin(angle)
        return np.stack(
            [np.concatenate([cosine, cosine], 1), np.concatenate([-sine, sine], 1)]
        ).astype(np.float32)

    return table(rows), table(GRID_W)


def kernel(
    nz,
    nt,
    heads,
    lat_in,
    ctx_hbm,
    cond,
    ctx_cond,
    mod_w,
    mod_b,
    qw,
    kw,
    vw,
    gw,
    low_hbm,
    decay_w,
    decay_b,
    extra,
    gain,
    out_w,
    final_g,
    final_b,
    row_hbm,
    col_hbm,
    out,
    L,
    XM,
    W,
    VG,
    WO,
    M,
    mod_part,
    PVG,
    PQK,
    QF,
    QD,
    O,
    U,
    TD,
    PF,
    OFF,
    LM,
    LR,
    CM,
    CR,
    DM,
    DR,
    RO,
    RR,
    SS,
    GT,
    GR,
    ACC,
    PS,
    PR,
    CX,
    LOWT,
    RT,
    CT,
    EC,
    EI,
    EO,
    loc_sem,
    once_s,
    once_r,
    wz_r,
    lx_r,
):
    z = lax.axis_index("sp")
    t = lax.axis_index("tp")
    share = nt // heads
    h = t // share
    p = t % share
    core = t % 2
    x = t // 2
    nx = nt // 2
    partner = t + 1 - 2 * core
    D = lat_in.shape[1]
    TB = lat_in.shape[0]
    tok = TB * nt
    KR = qw.shape[0]
    DK = qw.shape[1] // heads
    HC = DK // 2
    VC = vw.shape[1]
    MC = mod_w.shape[1]
    nb = tok // BLOCK
    dvs = VC // nz
    pending = []
    MP, MG, WZ, WD, LX, LD, WOUT, LMS, CMS, DMS, ROS, SSS, GRS, PRS = range(14)

    def push(src, dst, ssem, rsem, **where):
        pltpu.make_async_remote_copy(
            src_ref=src,
            dst_ref=dst,
            send_sem=ssem,
            recv_sem=rsem,
            device_id=where,
            device_id_type=pl.DeviceIdType.MESH,
        ).start()

    def waiter(view, ssem, rsem):
        return pltpu.make_async_remote_copy(
            src_ref=view,
            dst_ref=view,
            send_sem=ssem,
            recv_sem=rsem,
            device_id={"tp": partner},
            device_id_type=pl.DeviceIdType.MESH,
        )

    def all_in(kind, view):
        waiter(view, once_s.at[kind], once_r.at[kind]).wait_recv()

    def sent(kind, view):
        pending.append(waiter(view, once_s.at[kind], once_r.at[kind]))

    def far_first(n):
        return sorted(range(1, n), key=lambda i: (-min(i, n - i), i))

    def at_z(i):
        return lax.rem(z + i + nz, nz)

    def at_t(i):
        return lax.rem(t + i + nt, nt)

    def at_x(i):
        return lax.rem(x + i + nx, nx)

    def al(v, m):
        return pl.multiple_of(v, m)

    barrier = pltpu.get_barrier_semaphore()
    for i in range(1, nz):
        pl.semaphore_signal(
            barrier, inc=1, device_id={"sp": at_z(i)}, device_id_type=pl.DeviceIdType.MESH
        )
    for i in range(1, nt):
        pl.semaphore_signal(
            barrier, inc=1, device_id={"tp": at_t(i)}, device_id_type=pl.DeviceIdType.MESH
        )

    def w_at(zz, j, cc):
        return W.at[pl.ds(al(zz * KR, KR), KR), pl.ds(al(j * DK + cc * HC, HC), HC)]

    def l_at(xx, j, cc):
        return L.at[pl.ds(al((xx * 2 + cc) * TB, TB), TB), pl.ds(j * (D // 2), D // 2)]

    own_cols = pl.ds(al(h * DK + core * HC, HC), HC)
    local = [
        pltpu.make_async_copy(qw.at[:, own_cols], w_at(z, 0, core), loc_sem.at[0]),
        pltpu.make_async_copy(kw.at[:, own_cols], w_at(z, 1, core), loc_sem.at[1]),
        pltpu.make_async_copy(lat_in, L.at[pl.ds(al(t * TB, TB), TB), :], loc_sem.at[2]),
        pltpu.make_async_copy(vw, VG.at[:, pl.ds(0, VC)], loc_sem.at[3]),
        pltpu.make_async_copy(gw, VG.at[:, pl.ds(VC, VC)], loc_sem.at[4]),
        pltpu.make_async_copy(out_w, WO.at[pl.ds(al(p * VC, VC), VC), :], loc_sem.at[5]),
        pltpu.make_async_copy(ctx_hbm, CX, loc_sem.at[6]),
        pltpu.make_async_copy(low_hbm, LOWT, loc_sem.at[7]),
        pltpu.make_async_copy(row_hbm, RT, loc_sem.at[8]),
        pltpu.make_async_copy(col_hbm, CT, loc_sem.at[9]),
    ]
    for copy in local:
        copy.start()

    both = jnp.concatenate([cond[...], ctx_cond[...], jnp.zeros((6, cond.shape[1]), f32)], axis=0)
    part = dot(silu(both).astype(bf16), mod_w[...])
    mod_part[z] = part[0:2]

    for copy in local[:3]:
        copy.wait()
    pl.semaphore_wait(barrier, nz - 1 + nt - 1)

    for i in far_first(nz):
        push(mod_part.at[z], mod_part.at[z], once_s.at[MP], once_r.at[MP], sp=at_z(i))
    sent(MP, mod_part.at[pl.ds(0, nz - 1)])

    def ring(n, at, region, far, sem_r, kind, share_kind):
        long, short = n // 2, (n - 1) // 2

        def last(direction, j):
            return long if direction == j else short

        def index(direction, k, j):
            return (k - 1) * 4 + direction * 2 + j

        def send(direction, k, j):
            src = region(at(-k if direction == 0 else k), j, core)
            push(
                src,
                src,
                once_s.at[kind],
                sem_r.at[index(direction, k + 1, j)],
                **far(1 if direction == 0 else -1),
            )

        def give(xx, j):
            src = region(xx, j, core)
            push(src, src, once_s.at[share_kind], once_r.at[share_kind], tp=partner)

        def step(k):
            for j in range(2):
                for direction in range(2):
                    if 0 < k <= last(direction, j):
                        xx = at(-k if direction == 0 else k)
                        sem = sem_r.at[index(direction, k, j)]
                        waiter(region(xx, j, core), once_s.at[kind], sem).wait_recv()
                    if k < last(direction, j):
                        send(direction, k, j)
                for direction in range(2):
                    if 0 < k <= last(direction, j):
                        give(at(-k if direction == 0 else k), j)

        def start():
            step(0)

        def share_own():
            for j in range(2):
                give(at(0), j)

        return start, share_own, step, long

    l_start, l_own, l_step, l_last = ring(
        nx, at_x, l_at, lambda i: {"tp": at_x(i) * 2 + core}, lx_r, LX, LD
    )
    w_start, w_own, w_step, w_last = ring(nz, at_z, w_at, lambda i: {"sp": at_z(i)}, wz_r, WZ, WD)
    w_start()
    l_start()
    w_own()
    l_own()
    sent(WZ, W.at[pl.ds(0, (nz - 1) * KR), pl.ds(0, DK)])
    sent(WD, W.at[:, pl.ds(0, DK)])
    sent(LX, L.at[pl.ds(0, (nx - 1) * TB), :])
    sent(LD, L.at[pl.ds(0, nx * TB), :])

    def modulation_sums():
        all_in(MP, mod_part.at[pl.ds(0, nz - 1)])
        sums = mod_part[0]
        for i in range(1, nz):
            sums = sums + mod_part[i]
        cols = pl.ds(al(t * MC, 128), MC)
        M[:, cols] = sums
        for i in far_first(nt):
            push(M.at[:, cols], M.at[:, cols], once_s.at[MG], once_r.at[MG], tp=at_t(i))
        sent(MG, M.at[:, pl.ds(0, (nt - 1) * MC)])

    w_done = 0
    for k in range(1, l_last + 1):
        if k <= w_last:
            w_step(k)
            w_done = k
        l_step(k)
        if k == min(3, l_last):
            modulation_sums()
    local[5].wait()
    own_rows = WO.at[pl.ds(al(p * VC, VC), VC), :]
    for i in range(1, share):
        push(
            own_rows,
            own_rows,
            once_s.at[WOUT],
            once_r.at[WOUT],
            tp=h * share + lax.rem(p + i, share),
        )
    sent(WOUT, WO.at[pl.ds(0, (share - 1) * VC), :])
    all_in(LD, L.at[pl.ds(0, nx * TB), :])
    all_in(MG, M.at[:, pl.ds(0, (nt - 1) * MC)])
    for copy in local[3:5] + local[6:]:
        copy.wait()

    mod = M[...] + mod_b[...]
    shift, scale = mod[:, :D], 1.0 + mod[:, D : 2 * D]
    bias = decay_b[:, pl.ds(al(h * DK, DK), DK)]
    rank = decay_w.shape[1]
    zero = jnp.zeros((rank, DK), bf16)
    head_cols = pl.ds(al(h * DK, DK), DK)
    maps = [
        jnp.concatenate([decay_w[0, :, head_cols], zero], axis=0),
        jnp.concatenate([zero, decay_w[1, :, head_cols]], axis=0),
    ]

    def triangles(size):
        row = lax.broadcasted_iota(jnp.int32, (size, size), 0)
        col = lax.broadcasted_iota(jnp.int32, (size, size), 1)
        return row >= col, row <= col

    low_b, up_b = triangles(BLOCK)
    added = [extra[d, pl.ds(h, 1), :] for d in range(2)]

    def decays(low, d):
        return log_sigmoid(dot(low, maps[d]) + bias[d : d + 1]) * (1.0 / gate_scale)

    tiles = max(1, tok // 128)
    TR = tok // tiles

    def project_tile(i):
        rows = pl.ds(i * TR, TR)
        rounded = (L[rows, :].astype(f32) * scale[0:1] + shift[0:1]).astype(bf16)
        XM[rows, :] = rounded
        PVG[rows, :] = dot(rounded, VG[...]).astype(bf16)
        low = dot(rounded, LOWT[...], NT).astype(bf16)
        for d, mask in ((0, low_b), (1, up_b)):
            steps = decays(low, d)
            for b in range(i * TR // BLOCK, (i + 1) * TR // BLOCK):
                at = b * BLOCK - i * TR
                ex = added[d][:, b * BLOCK : (b + 1) * BLOCK]
                cum = dot(mask.astype(f32), steps[at : at + BLOCK], precision=highest) + jnp.sum(
                    jnp.where(mask, ex, 0.0), axis=1, keepdims=True
                )
                total = cum[BLOCK - 1 : BLOCK] if d == 0 else cum[0:1]
                block_rows = slice(b * BLOCK, (b + 1) * BLOCK)
                EC[d, block_rows, :] = jnp.exp(cum)
                EI[d, block_rows, :] = jnp.exp(-cum)
                EO[d, block_rows, :] = jnp.exp(total - cum)
                TD[d, b] = total

    tile = 0
    for k in range(w_done + 1, w_last + 1):
        if tile < tiles:
            project_tile(tile)
            tile += 1
        w_step(k)
    while tile < tiles:
        project_tile(tile)
        tile += 1

    ctx_rows = (CX[...].astype(f32) * scale[1:2] + shift[1:2]).astype(bf16)
    ctx_values = dot(ctx_rows, VG[:, 0:VC]).astype(bf16)
    ctx_low = dot(ctx_rows, LOWT[...], NT).astype(bf16)
    CB = ctx_hbm.shape[0]
    low_c, up_c = triangles(CB)
    cum_f = dot(low_c.astype(f32), decays(ctx_low, 0), precision=highest)
    cum_b = dot(up_c.astype(f32), decays(ctx_low, 1), precision=highest)
    tot_cf, tot_cb = cum_f[CB - 1 : CB], cum_b[0:1]
    sum_f, sum_b = jnp.zeros((1, DK), f32), jnp.zeros((1, DK), f32)
    for b in range(nb):
        OFF[0, b] = sum_f
        OFF[1, nb - 1 - b] = sum_b
        sum_f = sum_f + TD[0, b]
        sum_b = sum_b + TD[1, nb - 1 - b]
    DM[...] = jnp.concatenate([sum_f, sum_b, tot_cf, tot_cb], axis=0)
    for i in far_first(nz):
        push(DM, DR.at[z], once_s.at[DMS], once_r.at[DMS], sp=at_z(i))
    sent(DMS, DR.at[pl.ds(0, nz - 1)])
    DR[z] = DM[...]
    all_in(WD, W.at[:, pl.ds(0, DK)])

    def message(forward, backward):
        return jnp.concatenate(
            [forward.reshape(nz, dvs, DK), backward.reshape(nz, dvs, DK)], axis=1
        ).astype(bf16)

    ctx_keys = dot(ctx_rows, W[:, DK : 2 * DK]).astype(bf16).astype(f32)
    CM[...] = message(
        dot(ctx_values, (ctx_keys * jnp.exp(tot_cf - cum_f)).astype(bf16), TN),
        dot(ctx_values, (ctx_keys * jnp.exp(tot_cb - cum_b)).astype(bf16), TN),
    )
    for i in far_first(nz):
        push(CM.at[at_z(i)], CR.at[z], once_s.at[CMS], once_r.at[CMS], sp=at_z(i))
    sent(CMS, CM.at[pl.ds(0, nz - 1)])
    CR[z] = CM[z]

    QT = min(tok, 256)

    def project_qk(i, carry):
        rows = pl.ds(al(i * QT, QT), QT)
        PQK[rows, :] = dot(XM[rows, :], W[...]).astype(bf16)
        return carry

    lax.fori_loop(0, tok // QT, project_qk, 0)

    half = DK // 2
    for b in range(nb):
        rows = slice(b * BLOCK, (b + 1) * BLOCK)
        place = pl.ds(z * nb + b, 1)
        row_cos, row_sin = RT[0, place, :], RT[1, place, :]

        def rotated(values):
            first, second = values[:, :half], values[:, half:]
            return jnp.concatenate(
                [
                    first * row_cos + pltpu.roll(first, half // 2, 1) * row_sin,
                    second * CT[0] + pltpu.roll(second, half // 2, 1) * CT[1],
                ],
                axis=1,
            )

        q = rotated(PQK[rows, :DK].astype(f32)) * DK ** (-0.5)
        k = rotated(PQK[rows, DK:].astype(f32))
        v = PVG[rows, 0:VC]
        scores = None
        for d, mask in ((0, low_b), (1, up_b)):
            q_in = (q * EC[d, rows, :]).astype(bf16)
            k_in = (k * EI[d, rows, :]).astype(bf16)
            k_out = (k * EO[d, rows, :]).astype(bf16)
            QF[rows, d * DK : (d + 1) * DK] = q_in
            U[d, b] = dot(v, k_out, TN)
            one = jnp.where(mask, dot(q_in, k_in, NT), 0.0)
            scores = one if scores is None else scores + one
        O[rows, :] = dot(scores.astype(bf16), v)

    fwd, bwd = jnp.zeros((VC, DK), f32), jnp.zeros((VC, DK), f32)
    for b in range(nb):
        e = nb - 1 - b
        PF[0, b] = fwd.astype(bf16)
        PF[1, e] = bwd.astype(bf16)
        fwd = jnp.exp(TD[0, b]) * fwd + U[0, b]
        bwd = jnp.exp(TD[1, e]) * bwd + U[1, e]
    LM[...] = message(fwd, bwd)
    for i in far_first(nz):
        push(LM.at[at_z(i)], LR.at[z], once_s.at[LMS], once_r.at[LMS], sp=at_z(i))
    sent(LMS, LM.at[pl.ds(0, nz - 1)])
    LR[z] = LM[z]

    def inner(b, carry):
        rows = pl.ds(al(b * BLOCK, BLOCK), BLOCK)
        total = O[rows, :]
        for d in range(2):
            cols = slice(d * DK, (d + 1) * DK)
            q_in = QF[rows, cols]
            total = total + dot(q_in, PF[d, b], NT)
            QD[rows, cols] = (q_in.astype(f32) * jnp.exp(OFF[d, b])).astype(bf16)
        O[rows, :] = total
        return carry

    lax.fori_loop(0, nb, inner, 0)

    all_in(CMS, CR.at[pl.ds(0, nz - 1)])
    all_in(DMS, DR.at[pl.ds(0, nz - 1)])
    all_in(LMS, LR.at[pl.ds(0, nz - 1)])

    def context_chain(s, carry):
        fwd, bwd = carry
        e = nz - 1 - s
        fwd = jnp.exp(DR[s, 2:3]) * fwd + CR[s].astype(f32)[:dvs]
        bwd = jnp.exp(DR[e, 3:4]) * bwd + CR[e].astype(f32)[dvs:]
        return fwd, bwd

    slice0 = jnp.zeros((dvs, DK), f32)
    fwd, bwd = lax.fori_loop(0, nz, context_chain, (slice0, slice0))
    fwd_in, bwd_in = [], [None] * nz
    for s in range(nz):
        e = nz - 1 - s
        fwd_in.append(fwd)
        bwd_in[e] = bwd
        fwd = jnp.exp(DR[s, 0:1]) * fwd + LR[s].astype(f32)[:dvs]
        bwd = jnp.exp(DR[e, 1:2]) * bwd + LR[e].astype(f32)[dvs:]
    for s in range(nz):
        RO[s] = jnp.concatenate([fwd_in[s], bwd_in[s]], axis=0).astype(bf16)
    for i in far_first(nz):
        push(RO.at[at_z(i)], RR.at[z], once_s.at[ROS], once_r.at[ROS], sp=at_z(i))
    sent(ROS, RO.at[pl.ds(0, nz - 1)])
    RR[z] = RO[z]
    gate_rows = silu(PVG[:, VC:].astype(f32)) * gain[:, pl.ds(al(p * VC, VC), VC)]
    all_in(ROS, RR.at[pl.ds(0, nz - 1)])
    back = RR[...].astype(f32)
    start = jnp.concatenate(
        [back[:, :dvs].reshape(VC, DK), back[:, dvs:].reshape(VC, DK)], axis=1
    ).astype(bf16)
    mixture = O[...] + dot(QD[...], start, NT)

    SS[p] = dot(jnp.ones((8, VC), f32), mixture * mixture, NT, precision=highest)
    for i in range(1, share):
        push(
            SS.at[p],
            SS.at[p],
            once_s.at[SSS],
            once_r.at[SSS],
            tp=h * share + lax.rem(p + i, share),
        )
    sent(SSS, SS.at[pl.ds(0, share - 1)])
    unscaled = mixture * gate_rows
    all_in(SSS, SS.at[pl.ds(0, share - 1)])
    squares = SS[0]
    for i in range(1, share):
        squares = squares + SS[i]
    inverse = lax.rsqrt(squares / (share * VC) + norm_eps)
    gated = (unscaled * inverse.T[:, 0:1]).astype(bf16)
    GT[...] = gated.reshape(heads, share, TB, VC)
    for i in range(1, share):
        q = lax.rem(p + i, share)
        push(
            GT.at[:, q],
            GR.at[:, :, pl.ds(al(p * VC, VC), VC)],
            once_s.at[GRS],
            once_r.at[GRS],
            tp=h * share + q,
        )
    sent(GRS, GT.at[:, pl.ds(0, share - 1)])
    GR[:, :, pl.ds(al(p * VC, VC), VC)] = GT[:, p]
    all_in(WOUT, WO.at[pl.ds(0, (share - 1) * VC), :])
    all_in(GRS, GT.at[:, pl.ds(0, share - 1)])

    left = GR[...].reshape(heads * TB, share * VC)
    NC = D // 4
    for n in range(4):
        cols = slice(n * NC, (n + 1) * NC)
        partial = dot(left, WO[:, cols]).reshape(heads, TB, NC)
        ACC[:, :, cols] = partial
        PS[:, :, cols] = partial.astype(bf16)
    for i in range(1, heads):
        g = lax.rem(h + i, heads)
        push(PS.at[g], PR.at[h], once_s.at[PRS], once_r.at[PRS], tp=g * share + p)
    if heads > 1:
        sent(PRS, PS.at[pl.ds(0, heads - 1)])
        all_in(PRS, PR.at[pl.ds(0, heads - 1)])
    branch = ACC[h]
    for i in range(1, heads):
        g = lax.rem(h - i + heads, heads)
        branch = branch + PR[g].astype(f32)
    own = L[pl.ds(al(t * TB, TB), TB), :].astype(f32)
    gates = M[0:1, 2 * D :] + mod_b[:, 2 * D :]
    summed = residual_scale * own + gates * branch
    centered = summed - jnp.mean(summed, axis=1, keepdims=True)
    variance = jnp.mean(centered * centered, axis=1, keepdims=True)
    out[...] = (
        centered * lax.rsqrt(variance + norm_eps) * final_g[...] + final_b[...]
    ).astype(out.dtype)
    for copy in pending:
        copy.wait_send()


def body(
    nz,
    nt,
    latent,
    context,
    condition,
    context_condition,
    mod_weight,
    mod_bias,
    query_weight,
    key_weight,
    value_weight,
    out_gate_weight,
    decay_in_weight,
    decay_weight,
    decay_bias,
    extra_decay,
    norm_gain,
    out_weight,
    final_gain,
    final_bias,
):
    heads = ATTENTION_HEADS
    share = nt // heads
    D = latent.shape[1]
    TB = latent.shape[0]
    tok = TB * nt
    DK = query_weight.shape[1] // heads
    VC = value_weight.shape[1]
    MC = mod_weight.shape[1]
    nb = tok // BLOCK
    row_tab, col_tab = rotary_tables(nz * nb, DK // 2)
    dvs = VC // nz
    vmem = pl.BlockSpec(memory_space=pltpu.VMEM)
    hbm = pl.BlockSpec(memory_space=pl.ANY)
    dma = pltpu.SemaphoreType.DMA
    scratch = [
        pltpu.VMEM((tok, D), bf16),
        pltpu.VMEM((tok, D), bf16),
        pltpu.VMEM((D, 2 * DK), bf16),
        pltpu.VMEM((D, 2 * VC), bf16),
        pltpu.VMEM((share * VC, D), bf16),
        pltpu.VMEM((2, 3 * D), f32),
        pltpu.VMEM((nz, 2, MC), f32),
        pltpu.VMEM((tok, 2 * VC), bf16),
        pltpu.VMEM((tok, 2 * DK), bf16),
        pltpu.VMEM((tok, 2 * DK), bf16),
        pltpu.VMEM((tok, 2 * DK), bf16),
        pltpu.VMEM((tok, VC), f32),
        pltpu.VMEM((2, nb, VC, DK), f32),
        pltpu.VMEM((2, nb, 1, DK), f32),
        pltpu.VMEM((2, nb, VC, DK), bf16),
        pltpu.VMEM((2, nb, 1, DK), f32),
        pltpu.VMEM((nz, 2 * dvs, DK), bf16),
        pltpu.VMEM((nz, 2 * dvs, DK), bf16),
        pltpu.VMEM((nz, 2 * dvs, DK), bf16),
        pltpu.VMEM((nz, 2 * dvs, DK), bf16),
        pltpu.VMEM((4, DK), f32),
        pltpu.VMEM((nz, 4, DK), f32),
        pltpu.VMEM((nz, 2 * dvs, DK), bf16),
        pltpu.VMEM((nz, 2 * dvs, DK), bf16),
        pltpu.VMEM((share, 8, tok), f32),
        pltpu.VMEM((heads, share, TB, VC), bf16),
        pltpu.VMEM((heads, TB, share * VC), bf16),
        pltpu.VMEM((heads, TB, D), f32),
        pltpu.VMEM((heads, TB, D), bf16),
        pltpu.VMEM((heads, TB, D), bf16),
        pltpu.VMEM(context.shape, bf16),
        pltpu.VMEM((decay_in_weight.shape[1], D), bf16),
        pltpu.VMEM(row_tab.shape, f32),
        pltpu.VMEM(col_tab.shape, f32),
        pltpu.VMEM((2, tok, DK), f32),
        pltpu.VMEM((2, tok, DK), f32),
        pltpu.VMEM((2, tok, DK), f32),
        dma((10,)),
        dma((14,)),
        dma((14,)),
        dma((4 * (nz // 2),)),
        dma((4 * (nt // 4),)),
    ]
    in_specs = [vmem] * 20
    for index in (0, 1, 6, 7, 8, 9, 10, 15, 18, 19):
        in_specs[index] = hbm
    return pl.pallas_call(
        functools.partial(kernel, nz, nt, heads),
        out_shape=jax.ShapeDtypeStruct((TB, D), bf16),
        in_specs=in_specs,
        out_specs=vmem,
        scratch_shapes=scratch,
        compiler_params=pltpu.CompilerParams(
            collective_id=0, has_side_effects=True, vmem_limit_bytes=58 * 1024 * 1024
        ),
        name="layer",
    )(
        latent,
        context,
        condition.reshape(1, -1),
        context_condition.reshape(1, -1),
        mod_weight,
        mod_bias.reshape(1, -1),
        query_weight,
        key_weight,
        value_weight,
        out_gate_weight,
        decay_in_weight.T,
        decay_weight,
        decay_bias,
        extra_decay,
        norm_gain.reshape(1, -1),
        out_weight,
        final_gain.reshape(1, -1),
        final_bias.reshape(1, -1),
        jnp.asarray(row_tab),
        jnp.asarray(col_tab),
    )


def solution(mesh):
    placed = (
        P(("grp", "sp", "tp"), None),
        P(("grp", "sp"), None),
        P(("grp", "sp")),
        P("sp"),
        P("sp", "tp"),
        P(),
        P("sp", None),
        P("sp", None),
        P(None, "tp"),
        P(None, "tp"),
        P(),
        P(),
        P(),
        P(None, None, "sp"),
        P(),
        P("tp", None),
        P(),
        P(),
    )
    return jax.shard_map(
        functools.partial(body, mesh.shape["sp"], mesh.shape["tp"]),
        mesh=mesh,
        in_specs=placed,
        out_specs=P(("grp", "sp", "tp"), None),
        check_vma=False,
    )
```

time: 411 us -> 133 us (0.32)
  the two profiles are of different devices: /device:TPU:65 before, /device:TPU:83 now
where the time goes in v1:
time: 133 us
  Pallas kernels  131 us (98%)
  local copies, waits for them, and re-layouts  1.57 us (1%)
    pallas_call x1, Pallas kernels, body(): pl.pallas_call(functools.partial(kernel, nz, nt, heads), out_shape=jax.Sh...  131 us

profile of v1, /device:TPU:83, one launch (start us, length us, event | category | flops | bytes accessed | tf_op | source)
XLA Modules:
  0.0 132.7 jit_solution(6111547283815706478)
XLA Ops:
  0.0 131.1 %layer.1 = bf16[32,2048]{1,0:T(8,128)(2,1)} custom-call(bf16[32,2048]{1,0:T(8,128)(2,1)} %lat_in.1, bf16[32,2048]{1,0:T(8,128)(2,1)} %ctx_hbm.1, f32[1,128]{1,0:T(1,128)} %bitcast.12, f32[1,128]{1,0:T(1,128)} %bitcast.13, bf16[128,384]{1,0:T(8,128)(2,1)} %mod_w.1, f32[1,6144]{1,0:T(1,128)} %bitcast.8, bf16[128,1024]{1,0:T(8,128)(2,1)} %qw.1, ...), custom_call_target="tpu_custom_call" | custom-call | tf_op jit(solution)/shard_map/layer/pallas_call | solution.py:660
  131.1 1.6 %copy.22 = bf16[32,2048]{1,0:T(8,128)(2,1)} copy(bf16[32,2048]{1,0:T(8,128)(2,1)} %layer.1) | data formatting | bytes 262144

commit v2 on v1

--- a/solution.py
+++ b/solution.py
@@ -60,22 +60,22 @@
     heads,
     lat_in,
     ctx_hbm,
-    cond,
-    ctx_cond,
-    mod_w,
-    mod_b,
+    cond_hbm,
+    ctx_cond_hbm,
+    mod_w_hbm,
+    mod_b_hbm,
     qw,
     kw,
     vw,
     gw,
     low_hbm,
-    decay_w,
-    decay_b,
-    extra,
-    gain,
+    decay_w_hbm,
+    decay_b_hbm,
+    extra_hbm,
+    gain_hbm,
     out_w,
-    final_g,
-    final_b,
+    final_g_hbm,
+    final_b_hbm,
     row_hbm,
     col_hbm,
     out,
@@ -109,6 +109,17 @@
     ACC,
     PS,
     PR,
+    IV,
+    cond,
+    ctx_cond,
+    mod_w,
+    mod_b,
+    decay_w,
+    decay_b,
+    extra,
+    gain,
+    final_g,
+    final_b,
     CX,
     LOWT,
     RT,
@@ -138,7 +149,7 @@
     DK = qw.shape[1] // heads
     HC = DK // 2
     VC = vw.shape[1]
-    MC = mod_w.shape[1]
+    MC = mod_w_hbm.shape[1]
     nb = tok // BLOCK
     dvs = VC // nz
     pending = []
@@ -185,43 +196,58 @@
     def al(v, m):
         return pl.multiple_of(v, m)
 
+    def w_at(zz, j):
+        return W.at[pl.ds(al(zz * KR, KR), KR), pl.ds(j * DK, DK)]
+
+    def l_at(xx, j):
+        return L.at[pl.ds(al((xx * 2 + j) * TB, TB), TB), :]
+
+    head_cols = pl.ds(al(h * DK, DK), DK)
+    loads = [
+        (cond_hbm, cond),
+        (ctx_cond_hbm, ctx_cond),
+        (mod_w_hbm, mod_w),
+        (lat_in, L.at[pl.ds(al(t * TB, TB), TB), :]),
+        (qw.at[:, head_cols], w_at(z, 0)),
+        (kw.at[:, head_cols], w_at(z, 1)),
+        (out_w, WO.at[pl.ds(al(p * VC, VC), VC), :]),
+        (vw, VG.at[:, pl.ds(0, VC)]),
+        (gw, VG.at[:, pl.ds(VC, VC)]),
+        (ctx_hbm, CX),
+        (low_hbm, LOWT),
+        (mod_b_hbm, mod_b),
+        (decay_w_hbm, decay_w),
+        (decay_b_hbm, decay_b),
+        (extra_hbm, extra),
+        (gain_hbm, gain),
+        (final_g_hbm, final_g),
+        (final_b_hbm, final_b),
+        (row_hbm, RT),
+        (col_hbm, CT),
+    ]
+    local = [
+        pltpu.make_async_copy(src, dst, loc_sem.at[i]) for i, (src, dst) in enumerate(loads)
+    ]
+    for copy in local:
+        copy.start()
+
     barrier = pltpu.get_barrier_semaphore()
-    for i in range(1, nz):
+    for i in far_first(nz):
         pl.semaphore_signal(
             barrier, inc=1, device_id={"sp": at_z(i)}, device_id_type=pl.DeviceIdType.MESH
         )
-    for i in range(1, nt):
+    for i in far_first(nt):
         pl.semaphore_signal(
             barrier, inc=1, device_id={"tp": at_t(i)}, device_id_type=pl.DeviceIdType.MESH
         )
-
-    def w_at(zz, j, cc):
-        return W.at[pl.ds(al(zz * KR, KR), KR), pl.ds(al(j * DK + cc * HC, HC), HC)]
-
-    def l_at(xx, j, cc):
-        return L.at[pl.ds(al((xx * 2 + cc) * TB, TB), TB), pl.ds(j * (D // 2), D // 2)]
-
-    own_cols = pl.ds(al(h * DK + core * HC, HC), HC)
-    local = [
-        pltpu.make_async_copy(qw.at[:, own_cols], w_at(z, 0, core), loc_sem.at[0]),
-        pltpu.make_async_copy(kw.at[:, own_cols], w_at(z, 1, core), loc_sem.at[1]),
-        pltpu.make_async_copy(lat_in, L.at[pl.ds(al(t * TB, TB), TB), :], loc_sem.at[2]),
-        pltpu.make_async_copy(vw, VG.at[:, pl.ds(0, VC)], loc_sem.at[3]),
-        pltpu.make_async_copy(gw, VG.at[:, pl.ds(VC, VC)], loc_sem.at[4]),
-        pltpu.make_async_copy(out_w, WO.at[pl.ds(al(p * VC, VC), VC), :], loc_sem.at[5]),
-        pltpu.make_async_copy(ctx_hbm, CX, loc_sem.at[6]),
-        pltpu.make_async_copy(low_hbm, LOWT, loc_sem.at[7]),
-        pltpu.make_async_copy(row_hbm, RT, loc_sem.at[8]),
-        pltpu.make_async_copy(col_hbm, CT, loc_sem.at[9]),
-    ]
-    for copy in local:
-        copy.start()
+    for copy in local[:3]:
+        copy.wait()
 
     both = jnp.concatenate([cond[...], ctx_cond[...], jnp.zeros((6, cond.shape[1]), f32)], axis=0)
     part = dot(silu(both).astype(bf16), mod_w[...])
     mod_part[z] = part[0:2]
 
-    for copy in local[:3]:
+    for copy in local[3:6]:
         copy.wait()
     pl.semaphore_wait(barrier, nz - 1 + nt - 1)
 
@@ -239,7 +265,7 @@
             return (k - 1) * 4 + direction * 2 + j
 
         def send(direction, k, j):
-            src = region(at(-k if direction == 0 else k), j, core)
+            src = region(at(-k if direction == 0 else k), j)
             push(
                 src,
                 src,
@@ -249,7 +275,7 @@
             )
 
         def give(xx, j):
-            src = region(xx, j, core)
+            src = region(xx, j)
             push(src, src, once_s.at[share_kind], once_r.at[share_kind], tp=partner)
 
         def step(k):
@@ -258,34 +284,42 @@
                     if 0 < k <= last(direction, j):
                         xx = at(-k if direction == 0 else k)
                         sem = sem_r.at[index(direction, k, j)]
-                        waiter(region(xx, j, core), once_s.at[kind], sem).wait_recv()
+                        waiter(region(xx, j), once_s.at[kind], sem).wait_recv()
                     if k < last(direction, j):
                         send(direction, k, j)
                 for direction in range(2):
                     if 0 < k <= last(direction, j):
                         give(at(-k if direction == 0 else k), j)
 
-        def start():
-            step(0)
-
-        def share_own():
-            for j in range(2):
-                give(at(0), j)
-
-        return start, share_own, step, long
-
-    l_start, l_own, l_step, l_last = ring(
+        return send, give, step, long, last
+
+    l_send, l_give, l_step, l_long, l_last = ring(
         nx, at_x, l_at, lambda i: {"tp": at_x(i) * 2 + core}, lx_r, LX, LD
     )
-    w_start, w_own, w_step, w_last = ring(nz, at_z, w_at, lambda i: {"sp": at_z(i)}, wz_r, WZ, WD)
-    w_start()
-    l_start()
-    w_own()
-    l_own()
-    sent(WZ, W.at[pl.ds(0, (nz - 1) * KR), pl.ds(0, DK)])
-    sent(WD, W.at[:, pl.ds(0, DK)])
-    sent(LX, L.at[pl.ds(0, (nx - 1) * TB), :])
-    sent(LD, L.at[pl.ds(0, nx * TB), :])
+    w_send, w_give, w_step, w_long, w_last = ring(
+        nz, at_z, w_at, lambda i: {"sp": at_z(i)}, wz_r, WZ, WD
+    )
+    rest = pl.ds(0, (2 * nx - 1) * TB)
+
+    @pl.when(core == 0)
+    def _():
+        for direction in range(2):
+            if l_last(direction, 0):
+                l_send(direction, 0, 0)
+        l_give(x, 0)
+        all_in(LD, L.at[pl.ds(0, TB), :])
+        for direction in range(2):
+            if l_last(direction, 1):
+                l_send(direction, 0, 1)
+        for k in range(1, min(2, l_long) + 1):
+            l_step(k)
+
+    @pl.when(core == 1)
+    def _():
+        l_give(x, 1)
+        w_step(0)
+        for k in range(1, min(3, w_long) + 1):
+            w_step(k)
 
     def modulation_sums():
         all_in(MP, mod_part.at[pl.ds(0, nz - 1)])
@@ -298,15 +332,20 @@
             push(M.at[:, cols], M.at[:, cols], once_s.at[MG], once_r.at[MG], tp=at_t(i))
         sent(MG, M.at[:, pl.ds(0, (nt - 1) * MC)])
 
-    w_done = 0
-    for k in range(1, l_last + 1):
-        if k <= w_last:
+    modulation_sums()
+    w_done = min(5, w_long)
+
+    @pl.when(core == 0)
+    def _():
+        for k in range(3, l_long + 1):
+            l_step(k)
+
+    @pl.when(core == 1)
+    def _():
+        for k in range(4, w_done + 1):
             w_step(k)
-            w_done = k
-        l_step(k)
-        if k == min(3, l_last):
-            modulation_sums()
-    local[5].wait()
+
+    local[6].wait()
     own_rows = WO.at[pl.ds(al(p * VC, VC), VC), :]
     for i in range(1, share):
         push(
@@ -317,9 +356,12 @@
             tp=h * share + lax.rem(p + i, share),
         )
     sent(WOUT, WO.at[pl.ds(0, (share - 1) * VC), :])
-    all_in(LD, L.at[pl.ds(0, nx * TB), :])
+    @pl.when(core == 1)
+    def _():
+        all_in(LD, L.at[rest, :])
+
     all_in(MG, M.at[:, pl.ds(0, (nt - 1) * MC)])
-    for copy in local[3:5] + local[6:]:
+    for copy in local[7:]:
         copy.wait()
 
     mod = M[...] + mod_b[...]
@@ -327,7 +369,6 @@
     bias = decay_b[:, pl.ds(al(h * DK, DK), DK)]
     rank = decay_w.shape[1]
     zero = jnp.zeros((rank, DK), bf16)
-    head_cols = pl.ds(al(h * DK, DK), DK)
     maps = [
         jnp.concatenate([decay_w[0, :, head_cols], zero], axis=0),
         jnp.concatenate([zero, decay_w[1, :, head_cols]], axis=0),
@@ -369,11 +410,15 @@
                 TD[d, b] = total
 
     tile = 0
-    for k in range(w_done + 1, w_last + 1):
+    for k in range(w_done + 1, w_long + 1):
         if tile < tiles:
             project_tile(tile)
             tile += 1
-        w_step(k)
+
+        @pl.when(core == 1)
+        def _():
+            w_step(k)
+
     while tile < tiles:
         project_tile(tile)
         tile += 1
@@ -397,7 +442,9 @@
         push(DM, DR.at[z], once_s.at[DMS], once_r.at[DMS], sp=at_z(i))
     sent(DMS, DR.at[pl.ds(0, nz - 1)])
     DR[z] = DM[...]
-    all_in(WD, W.at[:, pl.ds(0, DK)])
+    @pl.when(core == 0)
+    def _():
+        all_in(WD, W.at[pl.ds(0, (nz - 1) * KR), :])
 
     def message(forward, backward):
         return jnp.concatenate(
@@ -523,45 +570,51 @@
             tp=h * share + lax.rem(p + i, share),
         )
     sent(SSS, SS.at[pl.ds(0, share - 1)])
-    unscaled = mixture * gate_rows
+    GT[...] = (mixture * gate_rows).reshape(nt, TB, VC)
+
+    def owner(q, j):
+        chip = jnp.where(q // 2 == 0, 2 * h - j + nx, 2 * h + 1 + j)
+        return lax.rem(chip, nx) * 2 + q % 2
+
+    lanes = pl.ds(al(p * VC, VC), VC)
+    for i in range(1, share):
+        q = lax.rem(p + i, share)
+        for j in range(heads):
+            push(
+                GT.at[owner(q, j)],
+                GR.at[j, :, lanes],
+                once_s.at[GRS],
+                once_r.at[GRS],
+                tp=h * share + q,
+            )
+    sent(GRS, GT.at[pl.ds(0, (share - 1) * heads)])
+    for j in range(heads):
+        GR[j, :, lanes] = GT[owner(p, j)]
     all_in(SSS, SS.at[pl.ds(0, share - 1)])
     squares = SS[0]
     for i in range(1, share):
         squares = squares + SS[i]
-    inverse = lax.rsqrt(squares / (share * VC) + norm_eps)
-    gated = (unscaled * inverse.T[:, 0:1]).astype(bf16)
-    GT[...] = gated.reshape(heads, share, TB, VC)
-    for i in range(1, share):
-        q = lax.rem(p + i, share)
-        push(
-            GT.at[:, q],
-            GR.at[:, :, pl.ds(al(p * VC, VC), VC)],
-            once_s.at[GRS],
-            once_r.at[GRS],
-            tp=h * share + q,
-        )
-    sent(GRS, GT.at[:, pl.ds(0, share - 1)])
-    GR[:, :, pl.ds(al(p * VC, VC), VC)] = GT[:, p]
+    IV[...] = lax.rsqrt(squares / (share * VC) + norm_eps).T.reshape(nt, TB, 8)
     all_in(WOUT, WO.at[pl.ds(0, (share - 1) * VC), :])
-    all_in(GRS, GT.at[:, pl.ds(0, share - 1)])
-
-    left = GR[...].reshape(heads * TB, share * VC)
+    all_in(GRS, GT.at[pl.ds(0, (share - 1) * heads)])
+
+    left = jnp.concatenate(
+        [(GR[j] * IV[owner(p, j)][:, 0:1]).astype(bf16) for j in range(heads)], axis=0
+    )
     NC = D // 4
     for n in range(4):
         cols = slice(n * NC, (n + 1) * NC)
         partial = dot(left, WO[:, cols]).reshape(heads, TB, NC)
-        ACC[:, :, cols] = partial
+        ACC[:, cols] = partial[0]
         PS[:, :, cols] = partial.astype(bf16)
-    for i in range(1, heads):
-        g = lax.rem(h + i, heads)
-        push(PS.at[g], PR.at[h], once_s.at[PRS], once_r.at[PRS], tp=g * share + p)
+    for j in range(heads - 1, 0, -1):
+        push(PS.at[j], PR.at[j], once_s.at[PRS], once_r.at[PRS], tp=owner(p, j))
+    branch = ACC[...]
     if heads > 1:
         sent(PRS, PS.at[pl.ds(0, heads - 1)])
         all_in(PRS, PR.at[pl.ds(0, heads - 1)])
-    branch = ACC[h]
-    for i in range(1, heads):
-        g = lax.rem(h - i + heads, heads)
-        branch = branch + PR[g].astype(f32)
+    for j in range(1, heads):
+        branch = branch + PR[j].astype(f32)
     own = L[pl.ds(al(t * TB, TB), TB), :].astype(f32)
     gates = M[0:1, 2 * D :] + mod_b[:, 2 * D :]
     summed = residual_scale * own + gates * branch
@@ -572,6 +625,18 @@
     ).astype(out.dtype)
     for copy in pending:
         copy.wait_send()
+
+    @pl.when(core == 0)
+    def _():
+        waiter(L.at[pl.ds(0, 2 * (nx - 1) * TB), :], once_s.at[LX], once_r.at[LX]).wait_send()
+        waiter(L.at[rest, :], once_s.at[LD], once_r.at[LD]).wait_send()
+
+    @pl.when(core == 1)
+    def _():
+        view = W.at[pl.ds(0, (nz - 1) * KR), :]
+        waiter(view, once_s.at[WZ], once_r.at[WZ]).wait_send()
+        waiter(view, once_s.at[WD], once_r.at[WD]).wait_send()
+        waiter(L.at[pl.ds(0, TB), :], once_s.at[LD], once_r.at[LD]).wait_send()
 
 
 def body(
@@ -636,11 +701,27 @@
         pltpu.VMEM((nz, 2 * dvs, DK), bf16),
         pltpu.VMEM((nz, 2 * dvs, DK), bf16),
         pltpu.VMEM((share, 8, tok), f32),
-        pltpu.VMEM((heads, share, TB, VC), bf16),
-        pltpu.VMEM((heads, TB, share * VC), bf16),
-        pltpu.VMEM((heads, TB, D), f32),
+        pltpu.VMEM((nt, TB, VC), f32),
+        pltpu.VMEM((heads, TB, share * VC), f32),
+        pltpu.VMEM((TB, D), f32),
         pltpu.VMEM((heads, TB, D), bf16),
         pltpu.VMEM((heads, TB, D), bf16),
+        pltpu.VMEM((nt, TB, 8), f32),
+        *[
+            pltpu.VMEM(shape, kind)
+            for shape, kind in (
+                ((1, condition.shape[0]), f32),
+                ((1, context_condition.shape[0]), f32),
+                (mod_weight.shape, bf16),
+                ((1, mod_bias.shape[0]), f32),
+                (decay_weight.shape, bf16),
+                (decay_bias.shape, f32),
+                (extra_decay.shape, f32),
+                ((1, norm_gain.shape[0]), f32),
+                ((1, D), f32),
+                ((1, D), f32),
+            )
+        ],
         pltpu.VMEM(context.shape, bf16),
         pltpu.VMEM((decay_in_weight.shape[1], D), bf16),
         pltpu.VMEM(row_tab.shape, f32),
@@ -648,15 +729,13 @@
         pltpu.VMEM((2, tok, DK), f32),
         pltpu.VMEM((2, tok, DK), f32),
         pltpu.VMEM((2, tok, DK), f32),
-        dma((10,)),
+        dma((20,)),
         dma((14,)),
         dma((14,)),
         dma((4 * (nz // 2),)),
         dma((4 * (nt // 4),)),
     ]
-    in_specs = [vmem] * 20
-    for index in (0, 1, 6, 7, 8, 9, 10, 15, 18, 19):
-        in_specs[index] = hbm
+    in_specs = [hbm] * 20
     return pl.pallas_call(
         functools.partial(kernel, nz, nt, heads),
         out_shape=jax.ShapeDtypeStruct((TB, D), bf16),

time: 133 us -> 128 us (0.962)
  the two profiles are of different devices: /device:TPU:83 before, /device:TPU:65 now
where the time goes in v2:
time: 128 us; the launch traced here: 127 us
  Pallas kernels  126 us (98%)
  local copies, waits for them, and re-layouts  1.57 us (1%)
    pallas_call x1, Pallas kernels, body(): pl.pallas_call(functools.partial(kernel, nz, nt, heads), out_shape=jax.Sh...  126 us

profile of v2, /device:TPU:65, one launch (start us, length us, event | category | flops | bytes accessed | tf_op | source)
XLA Modules:
  0.0 127.4 jit_solution(10573738848950696881)
XLA Ops:
  0.0 125.8 %layer.1 = bf16[32,2048]{1,0:T(8,128)(2,1)} custom-call(bf16[32,2048]{1,0:T(8,128)(2,1)} %lat_in.1, bf16[32,2048]{1,0:T(8,128)(2,1)} %ctx_hbm.1, f32[1,128]{1,0:T(1,128)} %bitcast.12, f32[1,128]{1,0:T(1,128)} %bitcast.13, bf16[128,384]{1,0:T(8,128)(2,1)} %mod_w_hbm.1, f32[1,6144]{1,0:T(1,128)} %bitcast.8, bf16[128,1024]{1,0:T(8,128)(2,1)} %qw.1, ...), custom_call_target="tpu_custom_call" | custom-call | tf_op jit(solution)/shard_map/layer/pallas_call | solution.py:739
  125.8 1.6 %copy.22 = bf16[32,2048]{1,0:T(8,128)(2,1)} copy(bf16[32,2048]{1,0:T(8,128)(2,1)} %layer.1) | data formatting | bytes 262144

commit v3 on v2

--- a/solution.py
+++ b/solution.py
@@ -52,6 +52,15 @@
         ).astype(np.float32)
 
     return table(rows), table(GRID_W)
+
+
+def spread(n, j):
+    long, short = n // 2, (n - 1) // 2
+    right, left = (long, short) if j % 2 == 0 else (short, long)
+    steps = {a: [a + 1] for a in range(1, right)} | {-a: [-a - 1] for a in range(1, left)}
+    steps[0] = ([1] if right else []) + ([-1] if left else [])
+    due = [o for a in range(1, long + 1) for o in (a, -a) if o <= right and o >= -left]
+    return due, steps
 
 
 def kernel(
@@ -87,6 +96,7 @@
     M,
     mod_part,
     PVG,
+    PLOW,
     PQK,
     QF,
     QD,
@@ -196,11 +206,14 @@
     def al(v, m):
         return pl.multiple_of(v, m)
 
-    def w_at(zz, j):
-        return W.at[pl.ds(al(zz * KR, KR), KR), pl.ds(j * DK, DK)]
+    def w_at(zz, j, parts=2):
+        rows = KR // parts
+        first = zz * KR + (j % parts) * rows
+        return W.at[pl.ds(al(first, rows), rows), pl.ds((j // parts) * DK, DK)]
 
     def l_at(xx, j):
-        return L.at[pl.ds(al((xx * 2 + j) * TB, TB), TB), :]
+        rows = pl.ds(al((xx * 2 + j // 2) * TB, TB), TB)
+        return L.at[rows, pl.ds((j % 2) * (D // 2), D // 2)]
 
     head_cols = pl.ds(al(h * DK, DK), DK)
     loads = [
@@ -208,8 +221,8 @@
         (ctx_cond_hbm, ctx_cond),
         (mod_w_hbm, mod_w),
         (lat_in, L.at[pl.ds(al(t * TB, TB), TB), :]),
-        (qw.at[:, head_cols], w_at(z, 0)),
-        (kw.at[:, head_cols], w_at(z, 1)),
+        (qw.at[:, head_cols], w_at(z, 0, 1)),
+        (kw.at[:, head_cols], w_at(z, 1, 1)),
         (out_w, WO.at[pl.ds(al(p * VC, VC), VC), :]),
         (vw, VG.at[:, pl.ds(0, VC)]),
         (gw, VG.at[:, pl.ds(VC, VC)]),
@@ -228,9 +241,6 @@
     local = [
         pltpu.make_async_copy(src, dst, loc_sem.at[i]) for i, (src, dst) in enumerate(loads)
     ]
-    for copy in local:
-        copy.start()
-
     barrier = pltpu.get_barrier_semaphore()
     for i in far_first(nz):
         pl.semaphore_signal(
@@ -240,6 +250,8 @@
         pl.semaphore_signal(
             barrier, inc=1, device_id={"tp": at_t(i)}, device_id_type=pl.DeviceIdType.MESH
         )
+    for copy in local:
+        copy.start()
     for copy in local[:3]:
         copy.wait()
 
@@ -255,71 +267,55 @@
         push(mod_part.at[z], mod_part.at[z], once_s.at[MP], once_r.at[MP], sp=at_z(i))
     sent(MP, mod_part.at[pl.ds(0, nz - 1)])
 
-    def ring(n, at, region, far, sem_r, kind, share_kind):
-        long, short = n // 2, (n - 1) // 2
-
-        def last(direction, j):
-            return long if direction == j else short
-
-        def index(direction, k, j):
-            return (k - 1) * 4 + direction * 2 + j
-
-        def send(direction, k, j):
-            src = region(at(-k if direction == 0 else k), j)
-            push(
-                src,
-                src,
-                once_s.at[kind],
-                sem_r.at[index(direction, k + 1, j)],
-                **far(1 if direction == 0 else -1),
-            )
-
-        def give(xx, j):
-            src = region(xx, j)
+    def ring(n, chunks, at, region, far, sem_r, kind, share_kind):
+        plans = [spread(n, j) for j in range(chunks)]
+
+        def give(o, j):
+            src = region(at(-o), j)
             push(src, src, once_s.at[share_kind], once_r.at[share_kind], tp=partner)
 
-        def step(k):
-            for j in range(2):
-                for direction in range(2):
-                    if 0 < k <= last(direction, j):
-                        xx = at(-k if direction == 0 else k)
-                        sem = sem_r.at[index(direction, k, j)]
-                        waiter(region(xx, j), once_s.at[kind], sem).wait_recv()
-                    if k < last(direction, j):
-                        send(direction, k, j)
-                for direction in range(2):
-                    if 0 < k <= last(direction, j):
-                        give(at(-k if direction == 0 else k), j)
-
-        return send, give, step, long, last
-
-    l_send, l_give, l_step, l_long, l_last = ring(
-        nx, at_x, l_at, lambda i: {"tp": at_x(i) * 2 + core}, lx_r, LX, LD
+        def hand_on(o, j):
+            src = region(at(-o), j)
+            for c in plans[j][1].get(o, []):
+                sem = sem_r.at[(c % n) * chunks + j]
+                push(src, src, once_s.at[kind], sem, **far(c - o))
+
+        def take(first, last):
+            for i in range(first, min(last, n - 1)):
+                for j in range(chunks):
+                    o = plans[j][0][i]
+                    sem = sem_r.at[(o % n) * chunks + j]
+                    waiter(region(at(-o), j), once_s.at[kind], sem).wait_recv()
+                    hand_on(o, j)
+                for j in range(chunks):
+                    give(plans[j][0][i], j)
+
+        return give, hand_on, take
+
+    l_give, l_on, l_take = ring(
+        nx, 4, at_x, l_at, lambda i: {"tp": at_x(i) * 2 + core}, lx_r, LX, LD
     )
-    w_send, w_give, w_step, w_long, w_last = ring(
-        nz, at_z, w_at, lambda i: {"sp": at_z(i)}, wz_r, WZ, WD
-    )
+    w_give, w_on, w_take = ring(nz, 4, at_z, w_at, lambda i: {"sp": at_z(i)}, wz_r, WZ, WD)
     rest = pl.ds(0, (2 * nx - 1) * TB)
 
     @pl.when(core == 0)
     def _():
-        for direction in range(2):
-            if l_last(direction, 0):
-                l_send(direction, 0, 0)
-        l_give(x, 0)
+        for j in range(2):
+            l_on(0, j)
+        for j in range(2):
+            l_give(0, j)
         all_in(LD, L.at[pl.ds(0, TB), :])
-        for direction in range(2):
-            if l_last(direction, 1):
-                l_send(direction, 0, 1)
-        for k in range(1, min(2, l_long) + 1):
-            l_step(k)
+        for j in range(2, 4):
+            l_on(0, j)
+        l_take(0, 4)
 
     @pl.when(core == 1)
     def _():
-        l_give(x, 1)
-        w_step(0)
-        for k in range(1, min(3, w_long) + 1):
-            w_step(k)
+        for j in range(2, 4):
+            l_give(0, j)
+        for j in range(4):
+            w_on(0, j)
+        w_take(0, 6)
 
     def modulation_sums():
         all_in(MP, mod_part.at[pl.ds(0, nz - 1)])
@@ -333,17 +329,14 @@
         sent(MG, M.at[:, pl.ds(0, (nt - 1) * MC)])
 
     modulation_sums()
-    w_done = min(5, w_long)
 
     @pl.when(core == 0)
     def _():
-        for k in range(3, l_long + 1):
-            l_step(k)
+        l_take(4, nx - 1)
 
     @pl.when(core == 1)
     def _():
-        for k in range(4, w_done + 1):
-            w_step(k)
+        w_take(6, 12)
 
     local[6].wait()
     own_rows = WO.at[pl.ds(al(p * VC, VC), VC), :]
@@ -356,10 +349,6 @@
             tp=h * share + lax.rem(p + i, share),
         )
     sent(WOUT, WO.at[pl.ds(0, (share - 1) * VC), :])
-    @pl.when(core == 1)
-    def _():
-        all_in(LD, L.at[rest, :])
-
     all_in(MG, M.at[:, pl.ds(0, (nt - 1) * MC)])
     for copy in local[7:]:
         copy.wait()
@@ -385,15 +374,33 @@
     def decays(low, d):
         return log_sigmoid(dot(low, maps[d]) + bias[d : d + 1]) * (1.0 / gate_scale)
 
+    @pl.when(core == 1)
+    def _():
+        all_in(LD, L.at[rest, :])
+
+    def context_decays():
+        ctx_rows = (CX[...].astype(f32) * scale[1:2] + shift[1:2]).astype(bf16)
+        ctx_values = dot(ctx_rows, VG[:, 0:VC]).astype(bf16)
+        ctx_low = dot(ctx_rows, LOWT[...], NT).astype(bf16)
+        CB = ctx_hbm.shape[0]
+        low_c, up_c = triangles(CB)
+        cum_f = dot(low_c.astype(f32), decays(ctx_low, 0), precision=highest)
+        cum_b = dot(up_c.astype(f32), decays(ctx_low, 1), precision=highest)
+        tot_cf, tot_cb = cum_f[CB - 1 : CB], cum_b[0:1]
+        return ctx_rows, ctx_values, cum_f, cum_b, tot_cf, tot_cb
+
     tiles = max(1, tok // 128)
     TR = tok // tiles
 
-    def project_tile(i):
+    def values_tile(i):
         rows = pl.ds(i * TR, TR)
         rounded = (L[rows, :].astype(f32) * scale[0:1] + shift[0:1]).astype(bf16)
         XM[rows, :] = rounded
         PVG[rows, :] = dot(rounded, VG[...]).astype(bf16)
-        low = dot(rounded, LOWT[...], NT).astype(bf16)
+        PLOW[rows, :] = dot(rounded, LOWT[...], NT).astype(bf16)
+
+    def decays_tile(i):
+        low = PLOW[pl.ds(i * TR, TR), :]
         for d, mask in ((0, low_b), (1, up_b)):
             steps = decays(low, d)
             for b in range(i * TR // BLOCK, (i + 1) * TR // BLOCK):
@@ -409,28 +416,17 @@
                 EO[d, block_rows, :] = jnp.exp(total - cum)
                 TD[d, b] = total
 
-    tile = 0
-    for k in range(w_done + 1, w_long + 1):
-        if tile < tiles:
-            project_tile(tile)
-            tile += 1
-
-        @pl.when(core == 1)
-        def _():
-            w_step(k)
-
-    while tile < tiles:
-        project_tile(tile)
-        tile += 1
-
-    ctx_rows = (CX[...].astype(f32) * scale[1:2] + shift[1:2]).astype(bf16)
-    ctx_values = dot(ctx_rows, VG[:, 0:VC]).astype(bf16)
-    ctx_low = dot(ctx_rows, LOWT[...], NT).astype(bf16)
-    CB = ctx_hbm.shape[0]
-    low_c, up_c = triangles(CB)
-    cum_f = dot(low_c.astype(f32), decays(ctx_low, 0), precision=highest)
-    cum_b = dot(up_c.astype(f32), decays(ctx_low, 1), precision=highest)
-    tot_cf, tot_cb = cum_f[CB - 1 : CB], cum_b[0:1]
+    pieces = [f for i in range(tiles) for f in ((values_tile, i), (decays_tile, i))]
+    for n, (piece, i) in enumerate(pieces):
+        piece(i)
+        if n < 3:
+            first, last = 12 + n, (13 + n if n + 1 < min(3, len(pieces)) else nz - 1)
+
+            @pl.when(core == 1)
+            def _():
+                w_take(first, last)
+
+    ctx_rows, ctx_values, cum_f, cum_b, tot_cf, tot_cb = context_decays()
     sum_f, sum_b = jnp.zeros((1, DK), f32), jnp.zeros((1, DK), f32)
     for b in range(nb):
         OFF[0, b] = sum_f
@@ -442,14 +438,15 @@
         push(DM, DR.at[z], once_s.at[DMS], once_r.at[DMS], sp=at_z(i))
     sent(DMS, DR.at[pl.ds(0, nz - 1)])
     DR[z] = DM[...]
-    @pl.when(core == 0)
-    def _():
-        all_in(WD, W.at[pl.ds(0, (nz - 1) * KR), :])
 
     def message(forward, backward):
         return jnp.concatenate(
             [forward.reshape(nz, dvs, DK), backward.reshape(nz, dvs, DK)], axis=1
         ).astype(bf16)
+
+    @pl.when(core == 0)
+    def _():
+        all_in(WD, W.at[pl.ds(0, (nz - 1) * KR), :])
 
     ctx_keys = dot(ctx_rows, W[:, DK : 2 * DK]).astype(bf16).astype(f32)
     CM[...] = message(
@@ -684,6 +681,7 @@
         pltpu.VMEM((2, 3 * D), f32),
         pltpu.VMEM((nz, 2, MC), f32),
         pltpu.VMEM((tok, 2 * VC), bf16),
+        pltpu.VMEM((tok, decay_in_weight.shape[1]), bf16),
         pltpu.VMEM((tok, 2 * DK), bf16),
         pltpu.VMEM((tok, 2 * DK), bf16),
         pltpu.VMEM((tok, 2 * DK), bf16),
@@ -732,8 +730,8 @@
         dma((20,)),
         dma((14,)),
         dma((14,)),
-        dma((4 * (nz // 2),)),
-        dma((4 * (nt // 4),)),
+        dma((4 * nz,)),
+        dma((2 * nt,)),
     ]
     in_specs = [hbm] * 20
     return pl.pallas_call(

time: 128 us -> 122 us (0.953)
  Pallas kernels: 126 us -> 120 us
    pallas_call x1, Pallas kernels: 126 us -> 120 us  [body(): pl.pallas_call(functools.partial(kernel, nz, nt, heads), out_shape=jax.Sh...]
where the time goes in v3:
time: 122 us
  Pallas kernels  120 us (98%)
  local copies, waits for them, and re-layouts  1.57 us (1%)
    pallas_call x1, Pallas kernels, body(): pl.pallas_call(functools.partial(kernel, nz, nt, heads), out_shape=jax.Sh...  120 us

profile of v3, /device:TPU:65, one launch (start us, length us, event | category | flops | bytes accessed | tf_op | source)
XLA Modules:
  0.0 121.9 jit_solution(15183909170316322780)
XLA Ops:
  0.0 120.3 %layer.1 = bf16[32,2048]{1,0:T(8,128)(2,1)} custom-call(bf16[32,2048]{1,0:T(8,128)(2,1)} %lat_in.1, bf16[32,2048]{1,0:T(8,128)(2,1)} %ctx_hbm.1, f32[1,128]{1,0:T(1,128)} %bitcast.12, f32[1,128]{1,0:T(1,128)} %bitcast.13, bf16[128,384]{1,0:T(8,128)(2,1)} %mod_w_hbm.1, f32[1,6144]{1,0:T(1,128)} %bitcast.8, bf16[128,1024]{1,0:T(8,128)(2,1)} %qw.1, ...), custom_call_target="tpu_custom_call" | custom-call | tf_op jit(solution)/shard_map/layer/pallas_call | solution.py:737
  120.3 1.6 %copy.22 = bf16[32,2048]{1,0:T(8,128)(2,1)} copy(bf16[32,2048]{1,0:T(8,128)(2,1)} %layer.1) | data formatting | bytes 262144

commit v4 on v3

--- a/solution.py
+++ b/solution.py
@@ -29,6 +29,22 @@
     if dims is None:
         dims = (((1,), (0,)), ((), ()))
     return lax.dot_general(a, b, dims, precision=precision, preferred_element_type=f32)
+
+
+def halves(a):
+    high = a.astype(bf16)
+    return high, (a - high.astype(f32)).astype(bf16)
+
+
+def dot2(a, b, dims=None):
+    high, low = halves(b)
+    return dot(a, high, dims) + dot(a, low, dims)
+
+
+def dot3(a, b, dims=None):
+    a_high, a_low = halves(a)
+    b_high, b_low = halves(b)
+    return dot(a_high, b_high, dims) + (dot(a_high, b_low, dims) + dot(a_low, b_high, dims))
 
 
 def log_sigmoid(v):
@@ -98,7 +114,7 @@
     PVG,
     PLOW,
     PQK,
-    QF,
+    QK,
     QD,
     O,
     U,
@@ -163,7 +179,7 @@
     nb = tok // BLOCK
     dvs = VC // nz
     pending = []
-    MP, MG, WZ, WD, LX, LD, WOUT, LMS, CMS, DMS, ROS, SSS, GRS, PRS = range(14)
+    MP, MG, WZ, WD, LX, LD, WOUT, LMS, CMS, DMS, ROS, SSS, GRS, PRS, DXS = range(15)
 
     def push(src, dst, ssem, rsem, **where):
         pltpu.make_async_remote_copy(
@@ -250,7 +266,7 @@
         pl.semaphore_signal(
             barrier, inc=1, device_id={"tp": at_t(i)}, device_id_type=pl.DeviceIdType.MESH
         )
-    for copy in local:
+    for copy in local[:6]:
         copy.start()
     for copy in local[:3]:
         copy.wait()
@@ -267,12 +283,8 @@
         push(mod_part.at[z], mod_part.at[z], once_s.at[MP], once_r.at[MP], sp=at_z(i))
     sent(MP, mod_part.at[pl.ds(0, nz - 1)])
 
-    def ring(n, chunks, at, region, far, sem_r, kind, share_kind):
+    def ring(n, chunks, at, region, whole, far, sem_r, kind, share_kind):
         plans = [spread(n, j) for j in range(chunks)]
-
-        def give(o, j):
-            src = region(at(-o), j)
-            push(src, src, once_s.at[share_kind], once_r.at[share_kind], tp=partner)
 
         def hand_on(o, j):
             src = region(at(-o), j)
@@ -287,34 +299,45 @@
                     sem = sem_r.at[(o % n) * chunks + j]
                     waiter(region(at(-o), j), once_s.at[kind], sem).wait_recv()
                     hand_on(o, j)
-                for j in range(chunks):
-                    give(plans[j][0][i], j)
-
-        return give, hand_on, take
-
-    l_give, l_on, l_take = ring(
-        nx, 4, at_x, l_at, lambda i: {"tp": at_x(i) * 2 + core}, lx_r, LX, LD
+                src = whole(at(-plans[0][0][i]))
+                push(src, src, once_s.at[share_kind], once_r.at[share_kind], tp=partner)
+
+        return hand_on, take
+
+    def l_whole(xx):
+        return L.at[pl.ds(al(xx * 2 * TB, 2 * TB), 2 * TB), :]
+
+    def w_whole(zz):
+        return W.at[pl.ds(al(zz * KR, KR), KR), :]
+
+    l_on, l_take = ring(
+        nx, 4, at_x, l_at, l_whole, lambda i: {"tp": at_x(i) * 2 + core}, lx_r, LX, LD
     )
-    w_give, w_on, w_take = ring(nz, 4, at_z, w_at, lambda i: {"sp": at_z(i)}, wz_r, WZ, WD)
+    w_on, w_take = ring(nz, 4, at_z, w_at, w_whole, lambda i: {"sp": at_z(i)}, wz_r, WZ, WD)
+    own_rows = L.at[pl.ds(al(t * TB, TB), TB), :]
     rest = pl.ds(0, (2 * nx - 1) * TB)
+
+    def load_rest():
+        for copy in local[6:]:
+            copy.start()
 
     @pl.when(core == 0)
     def _():
         for j in range(2):
             l_on(0, j)
-        for j in range(2):
-            l_give(0, j)
+        push(own_rows, own_rows, once_s.at[LD], once_r.at[LD], tp=partner)
         all_in(LD, L.at[pl.ds(0, TB), :])
         for j in range(2, 4):
             l_on(0, j)
+        load_rest()
         l_take(0, 4)
 
     @pl.when(core == 1)
     def _():
-        for j in range(2, 4):
-            l_give(0, j)
+        push(own_rows, own_rows, once_s.at[LD], once_r.at[LD], tp=partner)
         for j in range(4):
             w_on(0, j)
+        load_rest()
         w_take(0, 6)
 
     def modulation_sums():
@@ -339,11 +362,11 @@
         w_take(6, 12)
 
     local[6].wait()
-    own_rows = WO.at[pl.ds(al(p * VC, VC), VC), :]
+    proj_rows = WO.at[pl.ds(al(p * VC, VC), VC), :]
     for i in range(1, share):
         push(
-            own_rows,
-            own_rows,
+            proj_rows,
+            proj_rows,
             once_s.at[WOUT],
             once_r.at[WOUT],
             tp=h * share + lax.rem(p + i, share),
@@ -378,7 +401,12 @@
     def _():
         all_in(LD, L.at[rest, :])
 
-    def context_decays():
+    def message(forward, backward):
+        return jnp.concatenate(
+            [forward.reshape(nz, dvs, DK), backward.reshape(nz, dvs, DK)], axis=1
+        ).astype(bf16)
+
+    def context_states():
         ctx_rows = (CX[...].astype(f32) * scale[1:2] + shift[1:2]).astype(bf16)
         ctx_values = dot(ctx_rows, VG[:, 0:VC]).astype(bf16)
         ctx_low = dot(ctx_rows, LOWT[...], NT).astype(bf16)
@@ -387,7 +415,16 @@
         cum_f = dot(low_c.astype(f32), decays(ctx_low, 0), precision=highest)
         cum_b = dot(up_c.astype(f32), decays(ctx_low, 1), precision=highest)
         tot_cf, tot_cb = cum_f[CB - 1 : CB], cum_b[0:1]
-        return ctx_rows, ctx_values, cum_f, cum_b, tot_cf, tot_cb
+        DM[2] = tot_cf
+        DM[3] = tot_cb
+        ctx_keys = dot(ctx_rows, W[:, DK : 2 * DK]).astype(bf16).astype(f32)
+        CM[...] = message(
+            dot2(ctx_values, ctx_keys * jnp.exp(tot_cf - cum_f), TN),
+            dot2(ctx_values, ctx_keys * jnp.exp(tot_cb - cum_b), TN),
+        )
+        for i in far_first(nz):
+            push(CM.at[at_z(i)], CR.at[z], once_s.at[CMS], once_r.at[CMS], sp=at_z(i))
+        CR[z] = CM[z]
 
     tiles = max(1, tok // 128)
     TR = tok // tiles
@@ -425,38 +462,27 @@
             @pl.when(core == 1)
             def _():
                 w_take(first, last)
-
-    ctx_rows, ctx_values, cum_f, cum_b, tot_cf, tot_cb = context_decays()
+                if last == nz - 1:
+                    context_states()
+
+    @pl.when(core == 0)
+    def _():
+        all_in(WD, W.at[pl.ds(0, (nz - 1) * KR), :])
+        context_states()
+
     sum_f, sum_b = jnp.zeros((1, DK), f32), jnp.zeros((1, DK), f32)
     for b in range(nb):
         OFF[0, b] = sum_f
         OFF[1, nb - 1 - b] = sum_b
         sum_f = sum_f + TD[0, b]
         sum_b = sum_b + TD[1, nb - 1 - b]
-    DM[...] = jnp.concatenate([sum_f, sum_b, tot_cf, tot_cb], axis=0)
+    DM[0] = sum_f
+    DM[1] = sum_b
     for i in far_first(nz):
-        push(DM, DR.at[z], once_s.at[DMS], once_r.at[DMS], sp=at_z(i))
-    sent(DMS, DR.at[pl.ds(0, nz - 1)])
-    DR[z] = DM[...]
-
-    def message(forward, backward):
-        return jnp.concatenate(
-            [forward.reshape(nz, dvs, DK), backward.reshape(nz, dvs, DK)], axis=1
-        ).astype(bf16)
-
-    @pl.when(core == 0)
-    def _():
-        all_in(WD, W.at[pl.ds(0, (nz - 1) * KR), :])
-
-    ctx_keys = dot(ctx_rows, W[:, DK : 2 * DK]).astype(bf16).astype(f32)
-    CM[...] = message(
-        dot(ctx_values, (ctx_keys * jnp.exp(tot_cf - cum_f)).astype(bf16), TN),
-        dot(ctx_values, (ctx_keys * jnp.exp(tot_cb - cum_b)).astype(bf16), TN),
-    )
-    for i in far_first(nz):
-        push(CM.at[at_z(i)], CR.at[z], once_s.at[CMS], once_r.at[CMS], sp=at_z(i))
+        push(DM.at[p], DR.at[p, z], once_s.at[DMS], once_r.at[DMS], sp=at_z(i))
     sent(CMS, CM.at[pl.ds(0, nz - 1)])
-    CR[z] = CM[z]
+    sent(DMS, DR.at[0, pl.ds(0, nz - 1)])
+    DR[p, z] = DM[p]
 
     QT = min(tok, 256)
 
@@ -486,22 +512,16 @@
         q = rotated(PQK[rows, :DK].astype(f32)) * DK ** (-0.5)
         k = rotated(PQK[rows, DK:].astype(f32))
         v = PVG[rows, 0:VC]
-        scores = None
-        for d, mask in ((0, low_b), (1, up_b)):
-            q_in = (q * EC[d, rows, :]).astype(bf16)
-            k_in = (k * EI[d, rows, :]).astype(bf16)
-            k_out = (k * EO[d, rows, :]).astype(bf16)
-            QF[rows, d * DK : (d + 1) * DK] = q_in
-            U[d, b] = dot(v, k_out, TN)
-            one = jnp.where(mask, dot(q_in, k_in, NT), 0.0)
-            scores = one if scores is None else scores + one
-        O[rows, :] = dot(scores.astype(bf16), v)
+        QK[rows, :DK] = q
+        QK[rows, DK:] = k
+        for d in range(2):
+            U[d, b] = dot2(v, k * EO[d, rows, :], TN)
 
     fwd, bwd = jnp.zeros((VC, DK), f32), jnp.zeros((VC, DK), f32)
     for b in range(nb):
         e = nb - 1 - b
-        PF[0, b] = fwd.astype(bf16)
-        PF[1, e] = bwd.astype(bf16)
+        PF[0, b] = fwd
+        PF[1, e] = bwd
         fwd = jnp.exp(TD[0, b]) * fwd + U[0, b]
         bwd = jnp.exp(TD[1, e]) * bwd + U[1, e]
     LM[...] = message(fwd, bwd)
@@ -510,28 +530,41 @@
     sent(LMS, LM.at[pl.ds(0, nz - 1)])
     LR[z] = LM[z]
 
-    def inner(b, carry):
-        rows = pl.ds(al(b * BLOCK, BLOCK), BLOCK)
-        total = O[rows, :]
-        for d in range(2):
-            cols = slice(d * DK, (d + 1) * DK)
-            q_in = QF[rows, cols]
-            total = total + dot(q_in, PF[d, b], NT)
-            QD[rows, cols] = (q_in.astype(f32) * jnp.exp(OFF[d, b])).astype(bf16)
-        O[rows, :] = total
-        return carry
-
-    lax.fori_loop(0, nb, inner, 0)
+    for b in range(nb):
+        rows = slice(b * BLOCK, (b + 1) * BLOCK)
+        q, k = QK[rows, :DK], QK[rows, DK:]
+        scores = jnp.zeros((BLOCK, BLOCK), f32)
+        total = jnp.zeros((BLOCK, VC), f32)
+        for d, mask in ((0, low_b), (1, up_b)):
+            q_in = q * EC[d, rows, :]
+            scores = scores + jnp.where(mask, dot3(q_in, k * EI[d, rows, :], NT), 0.0)
+            total = total + dot3(q_in, PF[d, b], NT)
+            high, low = halves(q_in * jnp.exp(OFF[d, b]))
+            QD[0, rows, d * DK : (d + 1) * DK] = high
+            QD[1, rows, d * DK : (d + 1) * DK] = low
+        high, low = halves(scores)
+        v = PVG[rows, 0:VC]
+        O[rows, :] = total + (dot(high, v) + dot(low, v))
 
     all_in(CMS, CR.at[pl.ds(0, nz - 1)])
-    all_in(DMS, DR.at[pl.ds(0, nz - 1)])
+    all_in(DMS, DR.at[0, pl.ds(0, nz - 1)])
+    for i in range(1, share):
+        push(
+            DR.at[p],
+            DR.at[p],
+            once_s.at[DXS],
+            once_r.at[DXS],
+            tp=h * share + lax.rem(p + i, share),
+        )
+    sent(DXS, DR.at[pl.ds(0, share - 1)])
     all_in(LMS, LR.at[pl.ds(0, nz - 1)])
+    all_in(DXS, DR.at[pl.ds(0, share - 1)])
 
     def context_chain(s, carry):
         fwd, bwd = carry
         e = nz - 1 - s
-        fwd = jnp.exp(DR[s, 2:3]) * fwd + CR[s].astype(f32)[:dvs]
-        bwd = jnp.exp(DR[e, 3:4]) * bwd + CR[e].astype(f32)[dvs:]
+        fwd = jnp.exp(DR[2, s]) * fwd + CR[s].astype(f32)[:dvs]
+        bwd = jnp.exp(DR[3, e]) * bwd + CR[e].astype(f32)[dvs:]
         return fwd, bwd
 
     slice0 = jnp.zeros((dvs, DK), f32)
@@ -541,21 +574,23 @@
         e = nz - 1 - s
         fwd_in.append(fwd)
         bwd_in[e] = bwd
-        fwd = jnp.exp(DR[s, 0:1]) * fwd + LR[s].astype(f32)[:dvs]
-        bwd = jnp.exp(DR[e, 1:2]) * bwd + LR[e].astype(f32)[dvs:]
+        fwd = jnp.exp(DR[0, s]) * fwd + LR[s].astype(f32)[:dvs]
+        bwd = jnp.exp(DR[1, e]) * bwd + LR[e].astype(f32)[dvs:]
     for s in range(nz):
-        RO[s] = jnp.concatenate([fwd_in[s], bwd_in[s]], axis=0).astype(bf16)
+        RO[s] = jnp.concatenate([fwd_in[s], bwd_in[s]], axis=0)
     for i in far_first(nz):
         push(RO.at[at_z(i)], RR.at[z], once_s.at[ROS], once_r.at[ROS], sp=at_z(i))
     sent(ROS, RO.at[pl.ds(0, nz - 1)])
     RR[z] = RO[z]
     gate_rows = silu(PVG[:, VC:].astype(f32)) * gain[:, pl.ds(al(p * VC, VC), VC)]
     all_in(ROS, RR.at[pl.ds(0, nz - 1)])
-    back = RR[...].astype(f32)
-    start = jnp.concatenate(
-        [back[:, :dvs].reshape(VC, DK), back[:, dvs:].reshape(VC, DK)], axis=1
-    ).astype(bf16)
-    mixture = O[...] + dot(QD[...], start, NT)
+    back = RR[...]
+    start, start_low = halves(
+        jnp.concatenate([back[:, :dvs].reshape(VC, DK), back[:, dvs:].reshape(VC, DK)], axis=1)
+    )
+    mixture = O[...] + (
+        dot(QD[0], start, NT) + (dot(QD[0], start_low, NT) + dot(QD[1], start, NT))
+    )
 
     SS[p] = dot(jnp.ones((8, VC), f32), mixture * mixture, NT, precision=highest)
     for i in range(1, share):
@@ -600,18 +635,17 @@
     )
     NC = D // 4
     for n in range(4):
-        cols = slice(n * NC, (n + 1) * NC)
-        partial = dot(left, WO[:, cols]).reshape(heads, TB, NC)
-        ACC[:, cols] = partial[0]
-        PS[:, :, cols] = partial.astype(bf16)
-    for j in range(heads - 1, 0, -1):
-        push(PS.at[j], PR.at[j], once_s.at[PRS], once_r.at[PRS], tp=owner(p, j))
+        partial = dot(left, WO[:, n * NC : (n + 1) * NC]).reshape(heads, TB, NC)
+        ACC[:, n * NC : (n + 1) * NC] = partial[0]
+        PS[:, n] = partial.astype(bf16)
+        for j in range(heads - 1, 0, -1):
+            push(PS.at[j, n], PR.at[j, n], once_s.at[PRS], once_r.at[PRS], tp=owner(p, j))
     branch = ACC[...]
     if heads > 1:
         sent(PRS, PS.at[pl.ds(0, heads - 1)])
         all_in(PRS, PR.at[pl.ds(0, heads - 1)])
     for j in range(1, heads):
-        branch = branch + PR[j].astype(f32)
+        branch = branch + jnp.concatenate([PR[j, n].astype(f32) for n in range(4)], axis=1)
     own = L[pl.ds(al(t * TB, TB), TB), :].astype(f32)
     gates = M[0:1, 2 * D :] + mod_b[:, 2 * D :]
     summed = residual_scale * own + gates * branch
@@ -683,27 +717,27 @@
         pltpu.VMEM((tok, 2 * VC), bf16),
         pltpu.VMEM((tok, decay_in_weight.shape[1]), bf16),
         pltpu.VMEM((tok, 2 * DK), bf16),
-        pltpu.VMEM((tok, 2 * DK), bf16),
-        pltpu.VMEM((tok, 2 * DK), bf16),
+        pltpu.VMEM((tok, 2 * DK), f32),
+        pltpu.VMEM((2, tok, 2 * DK), bf16),
         pltpu.VMEM((tok, VC), f32),
         pltpu.VMEM((2, nb, VC, DK), f32),
         pltpu.VMEM((2, nb, 1, DK), f32),
-        pltpu.VMEM((2, nb, VC, DK), bf16),
+        pltpu.VMEM((2, nb, VC, DK), f32),
         pltpu.VMEM((2, nb, 1, DK), f32),
         pltpu.VMEM((nz, 2 * dvs, DK), bf16),
         pltpu.VMEM((nz, 2 * dvs, DK), bf16),
         pltpu.VMEM((nz, 2 * dvs, DK), bf16),
         pltpu.VMEM((nz, 2 * dvs, DK), bf16),
-        pltpu.VMEM((4, DK), f32),
-        pltpu.VMEM((nz, 4, DK), f32),
-        pltpu.VMEM((nz, 2 * dvs, DK), bf16),
-        pltpu.VMEM((nz, 2 * dvs, DK), bf16),
+        pltpu.VMEM((share, 1, DK), f32),
+        pltpu.VMEM((share, nz, 1, DK), f32),
+        pltpu.VMEM((nz, 2 * dvs, DK), f32),
+        pltpu.VMEM((nz, 2 * dvs, DK), f32),
         pltpu.VMEM((share, 8, tok), f32),
         pltpu.VMEM((nt, TB, VC), f32),
         pltpu.VMEM((heads, TB, share * VC), f32),
         pltpu.VMEM((TB, D), f32),
-        pltpu.VMEM((heads, TB, D), bf16),
-        pltpu.VMEM((heads, TB, D), bf16),
+        pltpu.VMEM((heads, 4, TB, D // 4), bf16),
+        pltpu.VMEM((heads, 4, TB, D // 4), bf16),
         pltpu.VMEM((nt, TB, 8), f32),
         *[
             pltpu.VMEM(shape, kind)
@@ -728,15 +762,15 @@
         pltpu.VMEM((2, tok, DK), f32),
         pltpu.VMEM((2, tok, DK), f32),
         dma((20,)),
-        dma((14,)),
-        dma((14,)),
+        dma((15,)),
+        dma((15,)),
         dma((4 * nz,)),
         dma((2 * nt,)),
     ]
     in_specs = [hbm] * 20
     return pl.pallas_call(
         functools.partial(kernel, nz, nt, heads),
-        out_shape=jax.ShapeDtypeStruct((TB, D), bf16),
+        out_shape=pltpu.VMEM((TB, D), bf16),
         in_specs=in_specs,
         out_specs=vmem,
         scratch_shapes=scratch,

time: 122 us -> 128 us (1.049)
  Pallas kernels: 120 us -> 127 us
    pallas_call x1, Pallas kernels: 120 us -> 127 us  [body(): pl.pallas_call(functools.partial(kernel, nz, nt, heads), out_shape=pltpu....]
where the time goes in v4:
time: 128 us
  Pallas kernels  127 us (99%)
    pallas_call x1, Pallas kernels, body(): pl.pallas_call(functools.partial(kernel, nz, nt, heads), out_shape=pltpu....  127 us

profile of v4, /device:TPU:65, one launch (start us, length us, event | category | flops | bytes accessed | tf_op | source)
XLA Modules:
  0.0 128.0 jit_solution(7092148220170918666)
XLA Ops:
  0.0 127.3 %layer.1 = bf16[32,2048]{1,0:T(8,128)(2,1)S(1)} custom-call(bf16[32,2048]{1,0:T(8,128)(2,1)} %lat_in.1, bf16[32,2048]{1,0:T(8,128)(2,1)} %ctx_hbm.1, f32[1,128]{1,0:T(1,128)} %bitcast.12, f32[1,128]{1,0:T(1,128)} %bitcast.13, bf16[128,384]{1,0:T(8,128)(2,1)} %mod_w_hbm.1, f32[1,6144]{1,0:T(1,128)} %bitcast.8, bf16[128,1024]{1,0:T(8,128)(2,1)} %qw.1, ...), custom_call_target="tpu_custom_call" | custom-call | tf_op jit(solution)/shard_map/layer/pallas_call | solution.py:771
  127.3 0.7 copy.22

commit v5 on v4

--- a/solution.py
+++ b/solution.py
@@ -415,8 +415,8 @@
         cum_f = dot(low_c.astype(f32), decays(ctx_low, 0), precision=highest)
         cum_b = dot(up_c.astype(f32), decays(ctx_low, 1), precision=highest)
         tot_cf, tot_cb = cum_f[CB - 1 : CB], cum_b[0:1]
-        DM[2] = tot_cf
-        DM[3] = tot_cb
+        DM[1, 0:1, :] = tot_cf
+        DM[1, 1:2, :] = tot_cb
         ctx_keys = dot(ctx_rows, W[:, DK : 2 * DK]).astype(bf16).astype(f32)
         CM[...] = message(
             dot2(ctx_values, ctx_keys * jnp.exp(tot_cf - cum_f), TN),
@@ -476,13 +476,13 @@
         OFF[1, nb - 1 - b] = sum_b
         sum_f = sum_f + TD[0, b]
         sum_b = sum_b + TD[1, nb - 1 - b]
-    DM[0] = sum_f
-    DM[1] = sum_b
+    DM[0, 0:1, :] = sum_f
+    DM[0, 1:2, :] = sum_b
     for i in far_first(nz):
-        push(DM.at[p], DR.at[p, z], once_s.at[DMS], once_r.at[DMS], sp=at_z(i))
+        push(DM.at[core], DR.at[core, z], once_s.at[DMS], once_r.at[DMS], sp=at_z(i))
     sent(CMS, CM.at[pl.ds(0, nz - 1)])
     sent(DMS, DR.at[0, pl.ds(0, nz - 1)])
-    DR[p, z] = DM[p]
+    DR[core, z] = DM[core]
 
     QT = min(tok, 256)
 
@@ -548,23 +548,16 @@
 
     all_in(CMS, CR.at[pl.ds(0, nz - 1)])
     all_in(DMS, DR.at[0, pl.ds(0, nz - 1)])
-    for i in range(1, share):
-        push(
-            DR.at[p],
-            DR.at[p],
-            once_s.at[DXS],
-            once_r.at[DXS],
-            tp=h * share + lax.rem(p + i, share),
-        )
-    sent(DXS, DR.at[pl.ds(0, share - 1)])
+    push(DR.at[core], DR.at[core], once_s.at[DXS], once_r.at[DXS], tp=partner)
+    sent(DXS, DR.at[0])
     all_in(LMS, LR.at[pl.ds(0, nz - 1)])
-    all_in(DXS, DR.at[pl.ds(0, share - 1)])
+    all_in(DXS, DR.at[0])
 
     def context_chain(s, carry):
         fwd, bwd = carry
         e = nz - 1 - s
-        fwd = jnp.exp(DR[2, s]) * fwd + CR[s].astype(f32)[:dvs]
-        bwd = jnp.exp(DR[3, e]) * bwd + CR[e].astype(f32)[dvs:]
+        fwd = jnp.exp(DR[1, s, 0:1]) * fwd + CR[s].astype(f32)[:dvs]
+        bwd = jnp.exp(DR[1, e, 1:2]) * bwd + CR[e].astype(f32)[dvs:]
         return fwd, bwd
 
     slice0 = jnp.zeros((dvs, DK), f32)
@@ -574,23 +567,21 @@
         e = nz - 1 - s
         fwd_in.append(fwd)
         bwd_in[e] = bwd
-        fwd = jnp.exp(DR[0, s]) * fwd + LR[s].astype(f32)[:dvs]
-        bwd = jnp.exp(DR[1, e]) * bwd + LR[e].astype(f32)[dvs:]
+        fwd = jnp.exp(DR[0, s, 0:1]) * fwd + LR[s].astype(f32)[:dvs]
+        bwd = jnp.exp(DR[0, e, 1:2]) * bwd + LR[e].astype(f32)[dvs:]
     for s in range(nz):
-        RO[s] = jnp.concatenate([fwd_in[s], bwd_in[s]], axis=0)
+        RO[s] = jnp.concatenate([fwd_in[s], bwd_in[s]], axis=0).astype(bf16)
     for i in far_first(nz):
         push(RO.at[at_z(i)], RR.at[z], once_s.at[ROS], once_r.at[ROS], sp=at_z(i))
     sent(ROS, RO.at[pl.ds(0, nz - 1)])
     RR[z] = RO[z]
     gate_rows = silu(PVG[:, VC:].astype(f32)) * gain[:, pl.ds(al(p * VC, VC), VC)]
     all_in(ROS, RR.at[pl.ds(0, nz - 1)])
-    back = RR[...]
-    start, start_low = halves(
-        jnp.concatenate([back[:, :dvs].reshape(VC, DK), back[:, dvs:].reshape(VC, DK)], axis=1)
-    )
-    mixture = O[...] + (
-        dot(QD[0], start, NT) + (dot(QD[0], start_low, NT) + dot(QD[1], start, NT))
-    )
+    back = RR[...].astype(f32)
+    start = jnp.concatenate(
+        [back[:, :dvs].reshape(VC, DK), back[:, dvs:].reshape(VC, DK)], axis=1
+    ).astype(bf16)
+    mixture = O[...] + (dot(QD[0], start, NT) + dot(QD[1], start, NT))
 
     SS[p] = dot(jnp.ones((8, VC), f32), mixture * mixture, NT, precision=highest)
     for i in range(1, share):
@@ -728,10 +719,10 @@
         pltpu.VMEM((nz, 2 * dvs, DK), bf16),
         pltpu.VMEM((nz, 2 * dvs, DK), bf16),
         pltpu.VMEM((nz, 2 * dvs, DK), bf16),
-        pltpu.VMEM((share, 1, DK), f32),
-        pltpu.VMEM((share, nz, 1, DK), f32),
-        pltpu.VMEM((nz, 2 * dvs, DK), f32),
-        pltpu.VMEM((nz, 2 * dvs, DK), f32),
+        pltpu.VMEM((2, 2, DK), f32),
+        pltpu.VMEM((2, nz, 2, DK), f32),
+        pltpu.VMEM((nz, 2 * dvs, DK), bf16),
+        pltpu.VMEM((nz, 2 * dvs, DK), bf16),
         pltpu.VMEM((share, 8, tok), f32),
         pltpu.VMEM((nt, TB, VC), f32),
         pltpu.VMEM((heads, TB, share * VC), f32),

time: 128 us -> 121 us (0.945)
  Pallas kernels: 127 us -> 120 us
    pallas_call x1, Pallas kernels: 127 us -> 120 us  [body(): pl.pallas_call(functools.partial(kernel, nz, nt, heads), out_shape=pltpu....]
where the time goes in v5:
time: 121 us
  Pallas kernels  120 us (99%)
    pallas_call x1, Pallas kernels, body(): pl.pallas_call(functools.partial(kernel, nz, nt, heads), out_shape=pltpu....  120 us

profile of v5, /device:TPU:65, one launch (start us, length us, event | category | flops | bytes accessed | tf_op | source)
XLA Modules:
  0.0 120.7 jit_solution(13366981658229503906)
XLA Ops:
  0.0 120.0 %layer.1 = bf16[32,2048]{1,0:T(8,128)(2,1)S(1)} custom-call(bf16[32,2048]{1,0:T(8,128)(2,1)} %lat_in.1, bf16[32,2048]{1,0:T(8,128)(2,1)} %ctx_hbm.1, f32[1,128]{1,0:T(1,128)} %bitcast.12, f32[1,128]{1,0:T(1,128)} %bitcast.13, bf16[128,384]{1,0:T(8,128)(2,1)} %mod_w_hbm.1, f32[1,6144]{1,0:T(1,128)} %bitcast.8, bf16[128,1024]{1,0:T(8,128)(2,1)} %qw.1, ...), custom_call_target="tpu_custom_call" | custom-call | tf_op jit(solution)/shard_map/layer/pallas_call | solution.py:762
  120.0 0.7 copy.22

commit v6 on v5

--- a/solution.py
+++ b/solution.py
@@ -583,7 +583,7 @@
     ).astype(bf16)
     mixture = O[...] + (dot(QD[0], start, NT) + dot(QD[1], start, NT))
 
-    SS[p] = dot(jnp.ones((8, VC), f32), mixture * mixture, NT, precision=highest)
+    SS[p] = dot(jnp.ones((8, VC), f32), mixture * mixture, NT, precision=highest)[0:1]
     for i in range(1, share):
         push(
             SS.at[p],
@@ -617,7 +617,8 @@
     squares = SS[0]
     for i in range(1, share):
         squares = squares + SS[i]
-    IV[...] = lax.rsqrt(squares / (share * VC) + norm_eps).T.reshape(nt, TB, 8)
+    inverse = lax.rsqrt(squares / (share * VC) + norm_eps)
+    IV[...] = jnp.broadcast_to(inverse, (8, tok)).T.reshape(nt, TB, 8)
     all_in(WOUT, WO.at[pl.ds(0, (share - 1) * VC), :])
     all_in(GRS, GT.at[pl.ds(0, (share - 1) * heads)])
 
@@ -723,7 +724,7 @@
         pltpu.VMEM((2, nz, 2, DK), f32),
         pltpu.VMEM((nz, 2 * dvs, DK), bf16),
         pltpu.VMEM((nz, 2 * dvs, DK), bf16),
-        pltpu.VMEM((share, 8, tok), f32),
+        pltpu.VMEM((share, 1, tok), f32),
         pltpu.VMEM((nt, TB, VC), f32),
         pltpu.VMEM((heads, TB, share * VC), f32),
         pltpu.VMEM((TB, D), f32),

time: 121 us -> 121 us (level)
  no operation moved by 1% of the time
where the time goes in v6:
time: 121 us; the launch traced here: 120 us
  Pallas kernels  120 us (99%)
    pallas_call x1, Pallas kernels, body(): pl.pallas_call(functools.partial(kernel, nz, nt, heads), out_shape=pltpu....  120 us

profile of v6, /device:TPU:65, one launch (start us, length us, event | category | flops | bytes accessed | tf_op | source)
XLA Modules:
  0.0 120.5 jit_solution(5877681758964009276)
XLA Ops:
  0.0 119.8 %layer.1 = bf16[32,2048]{1,0:T(8,128)(2,1)S(1)} custom-call(bf16[32,2048]{1,0:T(8,128)(2,1)} %lat_in.1, bf16[32,2048]{1,0:T(8,128)(2,1)} %ctx_hbm.1, f32[1,128]{1,0:T(1,128)} %bitcast.12, f32[1,128]{1,0:T(1,128)} %bitcast.13, bf16[128,384]{1,0:T(8,128)(2,1)} %mod_w_hbm.1, f32[1,6144]{1,0:T(1,128)} %bitcast.8, bf16[128,1024]{1,0:T(8,128)(2,1)} %qw.1, ...), custom_call_target="tpu_custom_call" | custom-call | tf_op jit(solution)/shard_map/layer/pallas_call | solution.py:763
  119.8 0.7 copy.22
